TPU v7x, 128 devices: a whole 4x4x4 slice. The times are simulated.
128 devices in a mesh: dp: 4 (over x), kv: 16 (over z, y), tp: 2 (over core).
Axes of the slice: x: 4, y: 4, z: 4, core: 2. Of those that a mesh axis runs over, the one named last changes fastest.
Arguments:
- tokens: bfloat16 [256, 4096], P('dp', 'kv'), may hold values from -6 to 6
- norm_gain: float32 [4096], P('kv'), may hold values from 0.1 to 1.9
- w_query: bfloat16 [4096, 2048], P('kv', 'tp'), may hold values from -0.09375 to 0.09375
- w_key: bfloat16 [4096, 2048], P('kv', 'tp'), may hold values from -0.09375 to 0.09375
- w_value: bfloat16 [4096, 2048], P('kv', 'tp'), may hold values from -0.09375 to 0.09375
- query_gain: float32 [64], replicated, may hold values from 0.1 to 1.9
- key_gain: float32 [64], replicated, may hold values from 0.1 to 1.9
- head_bias: float32 [32], P('tp'), may hold values from -11 to -3
- w_output: bfloat16 [2048, 4096], P('tp', 'kv'), may hold values from -0.125 to 0.125
- cache_keys: bfloat16 [16, 4096, 2048], P('dp', 'kv', 'tp'), may hold values from -6 to 6
- cache_values: bfloat16 [16, 4096, 2048], P('dp', 'kv', 'tp'), may hold values from -6 to 6
- base_length: int32 [16], P('dp'), may hold values from 3072 to 4064
- accepted: int32 [16], P('dp'), may hold values from 0 to 16
- parents: int32 [16, 16], P('dp'), may hold values from -1 to 14, as said below
Outputs:
- layer_out: bfloat16 [256, 4096], P('dp', 'kv')
- updated_keys: bfloat16 [16, 4096, 2048], P('dp', 'kv', 'tp')
- updated_values: bfloat16 [16, 4096, 2048], P('dp', 'kv', 'tp')
Inputs may be any that keep to these rules, and one draw needn't show every extreme that they name: base_length + accepted + 16 <= 4096 for every sequence. parents[s, i] is -1 or a proposal before i; parents[s, 0] is -1.
All inputs are finite; a program needn't handle non-finite values.
Results may differ from a plain program's by a relative error of at most 0.00175.
The roundings to bfloat16 on the way count: a program that leaves them out, or rounds other values in their place, can miss the bound.
Values may be sent and summed in bfloat16 or wider, within the bound.
No kernel may reach another device: no remote copies, remote signals or barrier semaphores. Data moves between devices by JAX's collectives and lax.ppermute only.
A program may use at most 64 MiB of HBM per device.

v0:
```python
import functools
import math

import jax
import jax.numpy as jnp
from jax import lax
from jax.sharding import Mesh
from jax.sharding import PartitionSpec as P

D = 4096
HEAD_DIM = 64
KV = ("kv_0", "kv_1")


epsilon = 1e-05


def split_up(x, dim, peers):
    shape = x.shape
    blocks = x.reshape(*shape[:dim], peers, shape[dim] // peers, *shape[dim + 1 :])
    return jnp.moveaxis(blocks, dim, 0)


def sent_and_summed(x, axis, dim):
    peers = lax.axis_size(axis)
    blocks = lax.all_to_all(split_up(x, dim, peers), axis, 0, 0, tiled=True)
    return jnp.sum(blocks, axis=0)


def in_one_piece(arrays, axis, dim, along):
    widths = [math.prod(a.shape[along:]) for a in arrays]
    both = jnp.concatenate(
        [a.reshape(*a.shape[:along], w) for a, w in zip(arrays, widths)], axis=along
    )
    filled = sent_and_summed(both, axis, dim)
    blocks = jnp.split(filled, [sum(widths[:k]) for k in range(1, len(widths))], axis=along)
    return tuple(
        (b.reshape(*filled.shape[:along], *a.shape[along:]) for a, b in zip(arrays, blocks))
    )


def sent_together(arrays, axis, dim, along):
    both = jnp.concatenate(arrays, axis=along)
    filled, at, gathered = (lax.all_gather(both, axis, axis=dim, tiled=True), 0, [])
    for a in arrays:
        gathered.append(lax.slice_in_dim(filled, at, at + a.shape[along], axis=along))
        at += a.shape[along]
    return tuple(gathered)


def copy_for_each(x, axis):
    copies = jnp.broadcast_to(x, (lax.axis_size(axis), *x.shape))
    return lax.all_to_all(copies, axis, split_axis=0, concat_axis=0, tiled=True)


def folded_in_pairs(pieces, combine):
    while len(jax.tree.leaves(pieces)[0]) > 1:
        pieces = jax.vmap(combine)(*(pieces[side::2] for side in (0, 1)))
    return pieces[0]


def entering(x, axis, combine, identity):
    peers, here = (lax.axis_size(axis), lax.axis_index(axis))
    passed = jnp.arange(peers) > here

    def kept(part, zero, own):
        part = jnp.where(
            passed.reshape(-1, *(1 for _ in own.shape)), part, jnp.asarray(zero, own.dtype)
        )
        return part[::-1]

    pieces = copy_for_each(x, axis)
    return folded_in_pairs(kept(pieces, identity, x), combine)


def over_pieces(x, axis):
    blocks = lax.all_gather(x, axis)
    return blocks.sum(axis=0)


def of_everyone(x, axis):
    return copy_for_each(x, axis).sum(axis=0)


def by_axis(x, axes):
    return functools.reduce(lax.psum, axes, x)


def head_norm(raw, gain):
    grouped = raw.reshape(raw.shape[0], -1, gain.shape[0])
    factor = lax.rsqrt(jnp.mean(grouped * grouped, axis=2, keepdims=True) + epsilon)
    return (grouped * factor * gain).reshape(raw.shape).astype(jnp.bfloat16)


def ancestry(parents):
    width = parents.shape[-1]
    direct = (parents[..., :, None] == jnp.arange(width, dtype=jnp.int32)).astype(jnp.float32)

    def extend(step, above):
        return direct + jnp.einsum("sij,sjk->sik", direct, above)

    return lax.fori_loop(0, width - 1, extend, direct)


def later_sum(values):
    length = values.shape[-1]
    order = jnp.arange(length, dtype=jnp.int32)
    after = (order[:, None] > order[None, :]).astype(jnp.float32)
    return jnp.einsum("shqp,pr->shqr", values, after, precision=lax.Precision.HIGHEST)


def finish(query_raw, key_raw, value_raw, squares, query_gain, key_gain):
    inv_rms = lax.rsqrt(squares / D + epsilon)
    queries = head_norm(query_raw, query_gain)
    new_keys = head_norm(key_raw, key_gain)
    new_values = (value_raw * inv_rms[:, None]).astype(jnp.bfloat16)
    return (queries, new_keys, new_values)


def shards(
    tokens,
    norm_gain,
    w_query,
    w_key,
    w_value,
    query_gain,
    key_gain,
    head_bias,
    w_output,
    cache_keys,
    cache_values,
    base_length,
    accepted,
    parents,
):
    wide = tokens.astype(jnp.float32)
    scaled = (wide * norm_gain).astype(jnp.bfloat16)
    squares = jnp.sum(wide * wide, axis=1)
    query_part = jnp.dot(scaled, w_query, preferred_element_type=jnp.float32)
    key_part = jnp.dot(scaled, w_key, preferred_element_type=jnp.float32)
    value_part = jnp.dot(scaled, w_value, preferred_element_type=jnp.float32)
    query_raw, key_raw, value_raw, row_squares = in_one_piece(
        (query_part, key_part, value_part, squares), KV, 0, 1
    )
    own_q, own_k, own_v = finish(query_raw, key_raw, value_raw, row_squares, query_gain, key_gain)
    queries, new_keys, new_values = sent_together((own_q, own_k, own_v), KV, 0, 1)
    seq_dev, width = parents.shape
    local_heads = head_bias.shape[0]
    span = cache_keys.shape[1]
    factor = HEAD_DIM ** (-0.5)
    shape_four = (seq_dev, width, local_heads, HEAD_DIM)
    query_heads = queries.reshape(shape_four)
    key_heads = new_keys.reshape(shape_four)
    value_heads = new_values.reshape(shape_four)
    stored_k = cache_keys.reshape(seq_dev, span, local_heads, HEAD_DIM)
    stored_v = cache_values.reshape(seq_dev, span, local_heads, HEAD_DIM)
    valid = base_length + accepted
    positions = lax.axis_index(KV) * span + jnp.arange(span, dtype=jnp.int32)
    live = (positions[None, :] < valid[:, None])[:, None, None, :]
    score = jnp.einsum("sqhd,sphd->shqp", query_heads, stored_k, preferred_element_type=jnp.float32)
    score = score * factor + head_bias[None, :, None, None]
    stay = jnp.where(live, jax.nn.log_sigmoid(-score), 0.0)
    tail = later_sum(stay)
    weight = jnp.where(live, jnp.exp(jax.nn.log_sigmoid(score) + tail), 0.0).astype(jnp.bfloat16)
    block_sum = jnp.einsum("shqp,sphd->sqhd", weight, stored_v, preferred_element_type=jnp.float32)
    block_log = jnp.sum(stay, axis=3)
    later = entering(block_log, KV, jnp.add, jnp.zeros_like(block_log))
    weighted = block_sum * jnp.exp(jnp.swapaxes(later, 1, 2))[..., None]
    cache_part = over_pieces(weighted, KV)
    mine = (ancestry(parents) > 0.5)[:, None, :, :]
    inner = jnp.einsum(
        "sqhd,sjhd->shqj", query_heads, key_heads, preferred_element_type=jnp.float32
    )
    inner = inner * factor + head_bias[None, :, None, None]
    stay_tree = jnp.where(mine, jax.nn.log_sigmoid(-inner), 0.0)
    tail_tree = later_sum(stay_tree)
    weight_tree = jnp.where(mine, jnp.exp(jax.nn.log_sigmoid(inner) + tail_tree), 0.0).astype(
        jnp.bfloat16
    )
    ancestor_sum = jnp.einsum(
        "shqj,sjhd->sqhd", weight_tree, value_heads, preferred_element_type=jnp.float32
    )
    ancestor_log = jnp.sum(stay_tree, axis=3)
    attended = ancestor_sum + jnp.exp(jnp.swapaxes(ancestor_log, 1, 2))[..., None] * cache_part
    attended = attended.astype(jnp.bfloat16).reshape(seq_dev * width, local_heads * HEAD_DIM)
    mix_part = jnp.dot(attended, w_output, preferred_element_type=jnp.float32)
    mix = of_everyone(mix_part, "tp")
    out_squares = by_axis(jnp.sum(mix * mix, axis=1), KV)
    layer_out = (mix * lax.rsqrt(out_squares / D + epsilon)[:, None]).astype(jnp.bfloat16)
    offset = positions[None, :] - valid[:, None]
    inside = ((offset >= 0) & (offset < width))[:, :, None]
    chooser = (offset[:, :, None] == jnp.arange(width, dtype=jnp.int32)).astype(jnp.bfloat16)
    fresh = jnp.concatenate(
        (new_keys.reshape(seq_dev, width, -1), new_values.reshape(seq_dev, width, -1)), axis=2
    )
    placed = jnp.einsum("spi,sic->spc", chooser, fresh, preferred_element_type=jnp.float32).astype(
        jnp.bfloat16
    )
    half = cache_keys.shape[2]
    updated_keys = jnp.where(inside, placed[:, :, :half], cache_keys)
    updated_values = jnp.where(inside, placed[:, :, half:], cache_values)
    return (layer_out, updated_keys, updated_values)


def solution(mesh):
    finer = Mesh(
        mesh.devices.reshape(mesh.shape["dp"], 4, 4, mesh.shape["tp"]), ("dp", "kv_0", "kv_1", "tp")
    )
    return jax.shard_map(
        shards,
        mesh=finer,
        in_specs=(
            P("dp", KV),
            P(KV),
            P(KV, "tp"),
            P(KV, "tp"),
            P(KV, "tp"),
            P(),
            P(),
            P("tp"),
            P("tp", KV),
            P("dp", KV, "tp"),
            P("dp", KV, "tp"),
            P("dp"),
            P("dp"),
            P("dp", None),
        ),
        out_specs=(P("dp", KV), P("dp", KV, "tp"), P("dp", KV, "tp")),
        check_vma=False,
    )
```

profile of v0, /device:TPU:0, one launch (start us, length us, event | category | flops | bytes accessed | tf_op | source)
XLA Modules:
  0.0 187.8 jit_solution(5200285393743870473)
XLA Ops:
  7.2 0.9 fusion.39
  8.2 1.0 fusion.48
  9.3 1.3 fusion.46
  10.7 0.9 fusion.44
  11.6 1.2 concatenate.20
  12.8 0.2 concatenate.25
  12.9 1.1 pad_maximum_fusion
  14.0 8.2 %all-to-all-start = ((f32[16,4,3073]{2,1,0:T(4,128)}), f32[16,4,3073]{2,1,0:T(4,128)S(1)}, u32[]{:S(2)}, u32[]{:S(2)}) async-start(f32[16,4,3073]{2,1,0:T(4,128)} %pad_maximum_fusion), calls=%async_computation | async-start | bytes 1638400 | tf_op jit(solution)/shard_map/all_to_all | solution.py:26
  22.4 2.5 %copy.79 = bf16[4,256,1024]{1,2,0:T(8,128)(2,1)} copy(bf16[4,256,1024]{2,1,0:T(8,128)(2,1)S(1)} %copy-done.1) | data formatting | bytes 4194304 | tf_op args[9]
  24.9 4.0 %copy.81 = bf16[4,256,1024]{1,2,0:T(8,128)(2,1)} copy(bf16[4,256,1024]{2,1,0:T(8,128)(2,1)} %param.26) | data formatting | bytes 4194304 | tf_op args[10]
  29.0 8.1 %all-to-all-done = f32[16,4,3073]{2,1,0:T(4,128)S(1)} async-done(((f32[16,4,3073]{2,1,0:T(4,128)}), f32[16,4,3073]{2,1,0:T(4,128)S(1)}, u32[]{:S(2)}, u32[]{:S(2)}) %all-to-all-start) | async-done | bytes 786720 | tf_op jit(solution)/shard_map/all_to_all | solution.py:26
  37.1 0.1 reduce_sum.82
  37.2 0.1 fusion.55
  38.2 21.6 %all-gather.1 = bf16[16,4,3072]{2,1,0:T(4,128)(2,1)S(1)} all-gather(bf16[1,4,3072]{2,1,0:T(4,128)(2,1)S(1)} %maximum_bitcast_fusion), channel_id=1, replica_groups=mesh['dp'=4,'kv_0'=4,'kv_1'=4,'tp'=2] {'kv_0','kv_1'}, dimensions={0}, use_global_device_ids=true | all-gather | bytes 417792 | tf_op jit(solution)/shard_map/all_gather | solution.py:44
  59.9 0.2 reshape.161
  60.1 2.1 %fusion.17 = (u16[4,16,256]{2,1,0:T(8,128)(2,1)S(1)}, f32[4,16,16,256]{3,2,1,0:T(8,128)S(1)}) fusion(f32[16]{0:T(128)S(1)} %copy-done.14, bf16[4,256,16,64]{1,3,2,0:T(8,128)(2,1)} %bitcast.49, bf16[4,16,16,64]{3,2,1,0:T(8,128)(2,1)S(1)} %reshape.161), kind=kOutput, calls=%fused_computation.33 | convolution fusion | flops 35373056 | bytes 3309632 | tf_op jit(solution)/shard_map/sqhd,sphd->shqp/dot_general | solution.py:160
  62.2 1.0 copy-done.4
  63.2 0.7 fusion.16
  64.0 0.9 reshape.174
  64.8 4.8 %all-to-all-start.1 = ((f32[16,1,1024]{2,1,0:T(1,128)}), f32[16,1,1024]{2,1,0:T(1,128)S(1)}, u32[]{:S(2)}, u32[]{:S(2)}) async-start(f32[16,1,1024]{2,1,0:T(1,128)} %reshape.174), calls=%async_computation.1 | async-start | bytes 131072 | tf_op jit(solution)/shard_map/all_to_all | solution.py:53
  69.6 0.2 all-gather.4.cloned.1.call-start
  69.8 4.2 %fusion.7 = bf16[4,16,16,256]{3,2,1,0:T(8,128)(2,1)} fusion(f32[4,16,16,256]{3,2,1,0:T(8,128)} %copy-done.4, pred[4,256]{1,0:T(4,128)(4,1)S(1)} %get-tuple-element.49, u16[4,16,256]{2,1,0:T(8,128)(2,1)S(1)} %get-tuple-element.52), kind=kOutput, calls=%fused_computation.15 | convolution fusion | flops 811139072 | bytes 1606656 | tf_op jit(solution)/shard_map/shqp,pr->shqr/dot_general | solution.py:109
  74.1 3.2 %all-to-all-done.1 = f32[16,1,1024]{2,1,0:T(1,128)S(1)} async-done(((f32[16,1,1024]{2,1,0:T(1,128)}), f32[16,1,1024]{2,1,0:T(1,128)S(1)}, u32[]{:S(2)}, u32[]{:S(2)}) %all-to-all-start.1) | async-done | bytes 65568 | tf_op jit(solution)/shard_map/all_to_all | solution.py:53
  77.3 0.5 broadcast.156
  77.8 0.8 reduce.6
  78.6 0.2 reshape.175
  78.8 0.1 broadcast_select_fusion
  79.1 1.3 copy-done.3
  80.5 0.7 fusion.11
  81.1 1.0 copy.82
  82.3 3.0 %while.11 = (s32[]{:T(128)}, f32[4,16,16]{2,1,0:T(8,128)S(1)}, s32[4,16]{1,0:T(4,128)S(1)}, s32[]{:T(128)}) while((s32[]{:T(128)}, f32[4,16,16]{2,1,0:T(8,128)S(1)}, s32[4,16]{1,0:T(4,128)S(1)}, s32[]{:T(128)}) %tuple.40), condition=%wide.region_5.6_spmd.clone, body=%wide.region_4.5_spmd.clone.sunk | while | flops 35842 | bytes 16693 | solution.py:102
  82.3 0.2 convolution_add_fusion.4
  82.5 0.2 convolution_add_fusion.4
  82.7 0.2 convolution_add_fusion.4
  82.9 0.2 convolution_add_fusion.4
  83.1 0.2 convolution_add_fusion.4
  83.3 0.2 convolution_add_fusion.4
  83.5 0.2 convolution_add_fusion.4
  83.7 0.2 convolution_add_fusion.4
  83.9 0.2 convolution_add_fusion.4
  84.1 0.2 convolution_add_fusion.4
  84.3 0.2 convolution_add_fusion.4
  84.5 0.2 convolution_add_fusion.4
  84.7 0.2 convolution_add_fusion.4
  84.9 0.2 convolution_add_fusion.4
  85.1 0.2 convolution_add_fusion.4
  85.5 0.9 reshape.162
  86.4 0.9 reshape.160
  87.3 1.2 fusion.23
  88.5 0.4 fusion.22
  89.0 1.1 fusion.13
  90.1 1.3 convolution_convert_fusion
  91.4 0.4 copy-done.2
  91.8 2.3 %slice_select_fusion = (bf16[4,256,1024]{2,1,0:T(8,128)(2,1)}, bf16[4,256,1024]{2,1,0:T(8,128)(2,1)}) fusion(bf16[4,256,1024]{2,1,0:T(8,128)(2,1)S(1)} %copy-done.2, bf16[4,256,2048]{2,1,0:T(8,128)(2,1)S(1)} %convolution_convert_fusion, pred[4,256]{1,0:T(4,128)(4,1)S(1)} %get-tuple-element.48, bf16[4,256,1024]{2,1,0:T(8,128)(2,1)S(1)} %copy-done.1), kind=kLoop, calls=%fused_computation.7 | loop fusion | flops 2097152 | bytes 12583936 | tf_op jit(solution)/shard_map/jit(_where)/select_n | solution.py:201
  94.1 57.6 %all-gather.4.cloned.1.call-done = f32[64,16,16,64]{3,2,1,0:T(8,128)} async-done(((f32[4,16,16,64]{3,2,1,0:T(8,128)}), f32[64,16,16,64]{3,2,1,0:T(8,128)}) %all-gather.4.cloned.1.call-update) | async-done | bytes 4194320 | tf_op jit(solution)/shard_map/all_gather | solution.py:77
  151.7 4.3 %reduce_sum.87 = f32[4,16,16,64]{3,2,1,0:T(8,128)S(1)} reduce(f32[16,4,16,16,64]{4,3,2,1,0:T(8,128)} %bitcast.47, f32[]{:T(128)} %constant.16.clone.1), dimensions={0}, to_apply=%region_8.9 | reduce | flops 983040 | bytes 4456452 | tf_op jit(solution)/shard_map/reduce_sum | solution.py:78
  156.0 0.4 fusion.14
  156.4 0.2 reshape.165
  156.6 0.4 copy-done.11
  157.0 0.2 fusion.63
  157.2 3.8 %all_to_all.15 = f32[2,64,256]{2,1,0:T(8,128)S(1)} all-to-all(f32[2,64,256]{2,1,0:T(8,128)S(1)} %broadcast_in_dim.89), channel_id=1, replica_groups=mesh['dp'=4,'kv_0'=4,'kv_1'=4,'tp'=2] {'tp'}, dimensions={0} | all-to-all | bytes 262144 | tf_op jit(solution)/shard_map/all_to_all | solution.py:53
  161.2 10.5 %psum.14 = f32[64]{0:T(128)S(1)} all-reduce(f32[64]{0:T(128)S(1)} %multiply_reduce_fusion), channel_id=1, replica_groups=mesh['dp'=4,'kv_0'=4,'kv_1'=4,'tp'=2] {'kv_0'}, use_global_device_ids=true, to_apply=%region_11.12 | all-reduce | flops 64 | bytes 512 | tf_op jit(solution)/shard_map/psum | solution.py:86
  171.7 8.5 %psum.15 = f32[64]{0:T(128)S(1)} all-reduce(f32[64]{0:T(128)S(1)} %psum.14), channel_id=1, replica_groups=mesh['dp'=4,'kv_0'=4,'kv_1'=4,'tp'=2] {'kv_1'}, use_global_device_ids=true, to_apply=%region_12.13 | all-reduce | flops 64 | bytes 512 | tf_op jit(solution)/shard_map/psum | solution.py:86
  180.2 0.7 multiply_convert_fusion
  (91 shorter events, 2.3 us)
Async XLA Ops:
  7.2 1.1 copy-start
  7.2 3.5 %copy-start.9 = (bf16[64,256]{1,0:T(8,128)(2,1)S(1)}, bf16[64,256]{1,0:T(8,128)(2,1)}, u32[]{:S(2)}) copy-start(bf16[64,256]{1,0:T(8,128)(2,1)} %param.16) | copy-start | bytes 98308
  7.2 3.5 %copy-start.13 = (f32[256]{0:T(256)S(1)}, f32[256]{0:T(256)}, u32[]{:S(2)}) copy-start(f32[256]{0:T(256)} %param.17) | copy-start | bytes 3076
  7.2 3.5 %copy-start.10 = (bf16[256,1024]{1,0:T(8,128)(2,1)S(1)}, bf16[256,1024]{1,0:T(8,128)(2,1)}, u32[]{:S(2)}) copy-start(bf16[256,1024]{1,0:T(8,128)(2,1)} %param.20) | copy-start | bytes 1572868
  11.6 10.6 %copy-start.15 = (f32[64]{0:T(128)S(1)}, f32[64]{0:T(128)}, u32[]{:S(2)}) copy-start(f32[64]{0:T(128)} %param.21) | copy-start | bytes 772
  11.6 10.7 %copy-start.16 = (f32[64]{0:T(128)S(1)}, f32[64]{0:T(128)}, u32[]{:S(2)}) copy-start(f32[64]{0:T(128)} %param.22) | copy-start | bytes 772
  11.6 10.8 %copy-start.1 = (bf16[4,256,1024]{2,1,0:T(8,128)(2,1)S(1)}, bf16[4,256,1024]{2,1,0:T(8,128)(2,1)}, u32[]{:S(2)}) copy-start(bf16[4,256,1024]{2,1,0:T(8,128)(2,1)} %param.25) | copy-start | bytes 6291460
  14.0 23.1 %all-to-all-start = ((f32[16,4,3073]{2,1,0:T(4,128)}), f32[16,4,3073]{2,1,0:T(4,128)S(1)}, u32[]{:S(2)}, u32[]{:S(2)}) async-start(f32[16,4,3073]{2,1,0:T(4,128)} %pad_maximum_fusion), calls=%async_computation | async-start | bytes 1638400 | tf_op jit(solution)/shard_map/all_to_all | solution.py:26
  24.9 4.0 %copy-start.17 = (s32[4]{0:T(128)S(1)}, s32[4]{0:T(128)}, u32[]{:S(2)}) copy-start(s32[4]{0:T(128)} %param.27) | copy-start | bytes 52
  24.9 4.0 %copy-start.18 = (s32[4]{0:T(128)S(1)}, s32[4]{0:T(128)}, u32[]{:S(2)}) copy-start(s32[4]{0:T(128)} %param.28) | copy-start | bytes 52
  28.9 31.2 %copy-start.14 = (f32[16]{0:T(128)S(1)}, f32[16]{0:T(128)}, u32[]{:S(2)}) copy-start(f32[16]{0:T(128)} %param.23) | copy-start | bytes 196
  60.1 2.1 %copy-start.5 = (bf16[4,16,16,64]{3,2,1,0:T(8,128)(2,1)}, bf16[4,16,16,64]{3,2,1,0:T(8,128)(2,1)S(1)}, u32[]{:S(2)}) copy-start(bf16[4,16,16,64]{3,2,1,0:T(8,128)(2,1)S(1)} %reshape.161) | copy-start | bytes 393220
  62.2 1.0 copy-start.4
  64.8 12.4 %all-to-all-start.1 = ((f32[16,1,1024]{2,1,0:T(1,128)}), f32[16,1,1024]{2,1,0:T(1,128)S(1)}, u32[]{:S(2)}, u32[]{:S(2)}) async-start(f32[16,1,1024]{2,1,0:T(1,128)} %reshape.174), calls=%async_computation.1 | async-start | bytes 131072 | tf_op jit(solution)/shard_map/all_to_all | solution.py:53
  69.6 82.1 %all-gather.4.cloned.1.call-start = ((), (), s32[]{:S(2)}) async-start(), calls=%async_computation.3 | async-start | bytes 8912896 | tf_op jit(solution)/shard_map/all_gather | solution.py:77
  78.8 1.6 copy-start.3
  78.8 1.7 copy-start.8
  80.5 1.7 copy-start.12
  81.1 6.2 %copy-start.6 = (bf16[4,16,16,64]{3,2,1,0:T(8,128)(2,1)S(1)}, bf16[4,16,16,64]{3,2,1,0:T(8,128)(2,1)}, u32[]{:S(2)}) copy-start(bf16[4,16,16,64]{3,2,1,0:T(8,128)(2,1)} %copy-done.5) | copy-start | bytes 393220
  90.1 1.8 copy-start.2
  151.7 4.3 %copy-start.7 = (bf16[4,16,16,64]{3,2,1,0:T(8,128)(2,1)S(1)}, bf16[4,16,16,64]{3,2,1,0:T(8,128)(2,1)}, u32[]{:S(2)}) copy-start(bf16[4,16,16,64]{3,2,1,0:T(8,128)(2,1)} %reshape.160) | copy-start | bytes 393220
  156.0 1.0 copy-start.11
Sparse Core Ops, SparseCore 0:
  82.3 69.3 all-gather.3
where the time goes:
time: 189 us; the launch traced here: 188 us
  waiting for transfers between devices  68.9 us (36%)
  blocking collectives  44.4 us (23%)
  local copies, waits for them, and re-layouts  17.2 us (9%)
  matrix products  17.2 us (9%)
  between operations  14.5 us (8%)
  starting transfers between devices  13.1 us (7%)
  other arithmetic  12.3 us (7%)
    all_gather x1, waiting for transfers between devices, over_pieces(): blocks = lax.all_gather(x, axis)  57.6 us
    all_gather x1, blocking collectives, sent_together(): lax.all_gather(both, axis, axis=dim, tiled=True)  21.6 us
    psum x2, blocking collectives, by_axis(): return functools.reduce(lax.psum, axes, x)  19 us
    unnamed x43, local copies, waits for them, and re-layouts  10.9 us
    all_to_all x1, starting transfers between devices, sent_and_summed(): blocks = lax.all_to_all(split_up(x, dim, peers), axis, 0, 0, tiled=True)  8.16 us
    all_to_all x1, waiting for transfers between devices, sent_and_summed(): blocks = lax.all_to_all(split_up(x, dim, peers), axis, 0, 0, tiled=True)  8.11 us
    dot_general x2, matrix products, later_sum(): jnp.einsum('shqp,pr->shqr', values, after, precision=lax.Precision.HIGHEST)  5.28 us
    all_to_all x1, starting transfers between devices, copy_for_each(): return lax.all_to_all(copies, axis, split_axis=0, concat_axis=0, tiled=True)  4.77 us
  transfers between devices with their start and end apart: 3, of which 3 were waited for; matrix products, arithmetic and copies ran while one was open for 12% of the time, Pallas kernels for 0%

commit v1 on v0

v1 whole, which is shorter than its diff:
```python
import functools

import jax
import jax.numpy as jnp
from jax import lax
from jax.experimental import pallas as pl
from jax.experimental.pallas import tpu as pltpu
from jax.sharding import Mesh
from jax.sharding import PartitionSpec as P

HEAD_DIM = 64
LANES = 128
KV = ("kv_0", "kv_1")
MIB = 1 << 20

epsilon = 1e-05
f32 = jnp.float32
bf16 = jnp.bfloat16


def low_half(rows):
    return lax.broadcasted_iota(jnp.int32, (rows, LANES), 1) < HEAD_DIM


def turned(x):
    return pltpu.roll(x, HEAD_DIM, 1)


def dot(a, b):
    return jnp.dot(a, b, preferred_element_type=f32)


def dot_nt(a, b):
    return lax.dot_general(a, b, (((1,), (1,)), ((), ())), preferred_element_type=f32)


def split_bf16(x, pieces):
    parts = []
    for _ in range(pieces):
        part = x.astype(bf16)
        parts.append(part)
        x = x - part.astype(f32)
    return parts


def signs(z):
    spill = jnp.log(1.0 + jnp.exp(-jnp.abs(z)))
    return -jnp.maximum(z, 0.0) - spill, jnp.minimum(z, 0.0) - spill


def project_kernel(tokens, gain, w_query, w_key, w_value, slots):
    rows, half = tokens.shape[0], tokens.shape[0] // 2
    wide = tokens[...].astype(f32)
    scaled = (wide * gain[...]).astype(bf16)
    low, low_v = low_half(rows), low_half(half)
    for at in range(0, w_query.shape[1], 2 * LANES):
        columns = pl.ds(at, 2 * LANES)
        query = dot(scaled, w_query[:, columns])
        key = dot(scaled, w_key[:, columns])
        value = dot(scaled, w_value[:, columns])
        for tile in range(2):
            head = at // HEAD_DIM + 2 * tile
            lanes = slice(tile * LANES, (tile + 1) * LANES)
            q, k, v = query[:, lanes], turned(key[:, lanes]), value[:, lanes]
            v_turned = turned(v)
            slots[head, :rows] = jnp.where(low, q, k)
            slots[head + 1, :rows] = jnp.where(low, k, q)
            slots[head, rows : rows + half] = jnp.where(low_v, v[:half], v_turned[half:])
            slots[head + 1, rows : rows + half] = jnp.where(low_v, v_turned[:half], v[half:])
    squares = wide * wide
    squares = jnp.concatenate((squares, jnp.zeros((LANES - rows, squares.shape[1]), f32)), axis=0)
    ones = jnp.ones((8, squares.shape[1]), bf16)
    row_squares = sum(dot_nt(ones, part) for part in split_bf16(squares, 3))
    for head in range(slots.shape[0]):
        slots[head, rows + half :] = row_squares


def normalize_kernel(width, place, got, query_gain, key_gain, slots, own):
    peers = got.shape[0]
    rows = got.shape[1] - 8
    half = rows // 3
    rows = 2 * half
    even = place[0] % 2 == 0
    total = got[0]
    for peer in range(1, peers):
        total = total + got[peer]
    both, value, squares = total[:rows], total[rows : rows + half], total[rows + half : rows + half + 1]
    low = low_half(rows)
    power = both * both
    low_sum = jnp.sum(jnp.where(low, power, 0.0), axis=1, keepdims=True)
    high_sum = jnp.sum(jnp.where(low, 0.0, power), axis=1, keepdims=True)
    factor = lax.rsqrt(jnp.where(low, low_sum, high_sum) / HEAD_DIM + epsilon)
    low_gain = jnp.where(even, query_gain[...], key_gain[...])
    high_gain = jnp.where(even, key_gain[...], query_gain[...])
    normed = (both * factor * jnp.where(low, low_gain, high_gain)).astype(bf16)
    inv_rms = jnp.broadcast_to(lax.rsqrt(squares / width + epsilon), (half, LANES))
    lane = lax.broadcasted_iota(jnp.int32, (half, LANES), 1)
    row = lax.broadcasted_iota(jnp.int32, (half, LANES), 0)
    first = jnp.sum(jnp.where(lane == row, inv_rms, 0.0), axis=1, keepdims=True)
    second = jnp.sum(jnp.where(lane == row + half, inv_rms, 0.0), axis=1, keepdims=True)
    fresh = (value * jnp.where(lane < HEAD_DIM, first, second)).astype(bf16)
    own[:rows] = normed
    own[rows:] = fresh
    for peer in range(peers):
        slots[peer, :rows] = normed
        slots[peer, rows:] = fresh


def tree_kernel(prop, place, bias, own, parents, out):
    half = own.shape[0] // 3
    rows = 2 * half
    even = place[0] % 2 == 0
    low = low_half(rows)
    both = own[:rows].astype(f32)
    other = turned(both)
    query = jnp.where(low, jnp.where(even, both, other), 0.0).astype(bf16)
    key = jnp.where(even, other, both).astype(bf16)
    score = dot_nt(query, key) * HEAD_DIM ** (-0.5) + bias[place[0]]
    row = lax.broadcasted_iota(jnp.int32, (rows, rows), 0)
    column = lax.broadcasted_iota(jnp.int32, (rows, rows), 1)
    parent = parents[...]
    direct = (parent >= 0) & (column == row - row % prop + parent)
    step = jnp.where(direct, 1.0, 0.0).astype(bf16)
    above = jnp.where(row == column, 1.0, 0.0)
    above = above + step.astype(f32)
    reach = 2
    while reach < prop:
        step = dot(step, step).astype(bf16)
        above = above + dot(above.astype(bf16), step)
        reach *= 2
    mine = (above > 0.5) & (row != column)
    stay, taken = signs(score)
    stay = jnp.where(mine, stay, 0.0)
    after = jnp.where(row > column, 1.0, 0.0).astype(bf16)
    tail = sum(dot(part, after) for part in split_bf16(stay, 3))
    weight = jnp.where(mine, jnp.exp(taken + tail), 0.0).astype(bf16)
    kept = jnp.exp(jnp.sum(stay, axis=1, keepdims=True))
    value = own[rows:].astype(f32)
    value = jnp.concatenate((value, turned(value)), axis=0).astype(bf16)
    summed = dot(weight, value)
    low = low_half(half)
    out[0] = jnp.where(low, summed[:half], turned(summed[half:]))
    out[1] = jnp.where(low, kept[:half], kept[half:])


def attend_kernel(prop, place, valid, bias, fresh, keys, values, slots):
    seqs, span, _ = keys.shape
    heads = fresh.shape[0]
    rows = seqs * prop
    group = 4
    tall = heads * prop
    low = low_half(prop)
    low_mask = low.astype(f32).astype(bf16)
    high_mask = (1.0 - low.astype(f32)).astype(bf16)
    blank = jnp.zeros((prop, LANES), bf16)
    order = lax.broadcasted_iota(jnp.int32, (span, span), 0)
    after = jnp.where(order > lax.broadcasted_iota(jnp.int32, (span, span), 1), 1.0, 0.0).astype(bf16)
    position = place[0] * span + lax.broadcasted_iota(jnp.int32, (1, span), 1)
    quarter = lax.broadcasted_iota(jnp.int32, (prop, LANES), 1) // (LANES // seqs)
    sums, logs = [], []
    for seq in range(seqs):
        live = position < valid[seq]
        scores = []
        for first in range(0, heads, group):
            blocks = []
            for j in range(group):
                tile = fresh[first + j, seq * prop : (seq + 1) * prop] * (low_mask if j % 2 == 0 else high_mask)
                blocks.append(jnp.concatenate((tile, blank) if j < 2 else (blank, tile), axis=1))
            stored = keys[seq, :, first * HEAD_DIM : (first + group) * HEAD_DIM]
            score = dot_nt(jnp.concatenate(blocks, axis=0), stored)
            for j in range(group):
                part = score[j * prop : (j + 1) * prop]
                scores.append(part * HEAD_DIM ** (-0.5) + bias[first + j])
        stay, taken = signs(jnp.concatenate(scores, axis=0))
        stay = jnp.where(live, stay, 0.0)
        tail = dot(jnp.concatenate(split_bf16(stay, 2), axis=0), after)
        tail = tail[:tall] + tail[tall:]
        weight = jnp.where(live, jnp.exp(taken + tail), 0.0).astype(bf16)
        logs.append(tail[:, :1] + stay[:, :1])
        tiles = []
        for first in range(0, heads, group):
            stored = values[seq, :, first * HEAD_DIM : (first + group) * HEAD_DIM]
            summed = dot(weight[first * prop : (first + group) * prop], stored)
            for j in range(group):
                lanes = slice(j // 2 * LANES, (j // 2 + 1) * LANES)
                tiles.append(summed[j * prop : (j + 1) * prop, lanes])
        sums.append(tiles)
    for head in range(heads):
        for seq in range(seqs // 2):
            one, two = sums[seq][head], sums[seq + seqs // 2][head]
            one, two = (one, turned(two)) if head % 2 == 0 else (turned(one), two)
            slots[head, seq * prop : (seq + 1) * prop] = jnp.where(low, one, two)
        log = jnp.zeros((prop, LANES), f32)
        for seq in range(seqs):
            log = jnp.where(quarter == seq, logs[seq][head * prop : (head + 1) * prop], log)
        slots[head, rows // 2 :] = log


def combine_kernel(got, tree, slots):
    blocks, tall, _ = got.shape
    prop = tall // 3
    half = 2 * prop
    lane = lax.broadcasted_iota(jnp.int32, (prop, LANES), 1)
    first = lane % HEAD_DIM < HEAD_DIM // 2
    later = jnp.zeros((prop, LANES), f32)
    part = jnp.zeros((half, LANES), f32)
    for block in range(blocks - 1, -1, -1):
        kept = jnp.exp(later)
        one = jnp.where(first, kept, pltpu.roll(kept, HEAD_DIM // 2, 1))
        two = jnp.where(first, pltpu.roll(kept, LANES - HEAD_DIM // 2, 1), kept)
        part = part + jnp.concatenate((one, two), axis=0) * got[block, :half]
        later = later + got[block, half:]
    attended = (tree[0] + tree[1] * part).astype(bf16)
    for block in range(blocks):
        slots[block] = attended


def output_kernel(got, w_output, out):
    heads, half, _ = got.shape
    low = low_half(half)
    columns = []
    for head in range(0, heads, 2):
        one, two = got[head].astype(f32), got[head + 1].astype(f32)
        top = jnp.where(low, one, turned(two))
        bottom = jnp.where(low, turned(one), two)
        columns.append(jnp.concatenate((top, bottom), axis=0).astype(bf16))
    out[...] = dot(jnp.concatenate(columns, axis=1), w_output[...])


def squares_kernel(one, two, mix, slots):
    total = one[...] + two[...]
    mix[...] = total
    rows = total.shape[0]
    squares = jnp.sum(total * total, axis=1, keepdims=True)
    lane = lax.broadcasted_iota(jnp.int32, (rows, LANES), 1)
    row = lax.broadcasted_iota(jnp.int32, (rows, LANES), 0)
    flat = jnp.sum(jnp.where(lane == row, squares, 0.0), axis=0, keepdims=True)
    slots[...] = jnp.broadcast_to(flat[None], slots.shape)


def finish_kernel(width, mix, got, out):
    total = got[0]
    for peer in range(1, got.shape[0]):
        total = total + got[peer]
    rows = out.shape[0]
    factor = jnp.broadcast_to(lax.rsqrt(total[:1] / width + epsilon), (rows, LANES))
    lane = lax.broadcasted_iota(jnp.int32, (rows, LANES), 1)
    row = lax.broadcasted_iota(jnp.int32, (rows, LANES), 0)
    factor = jnp.sum(jnp.where(lane == row, factor, 0.0), axis=1, keepdims=True)
    out[...] = (mix[...] * factor).astype(bf16)


def update_kernel(prop, place, valid, fresh, keys, values, new_keys, new_values):
    seq = pl.program_id(0)
    _, span, _ = keys.shape
    heads = fresh.shape[0]
    rows = 2 * (fresh.shape[1] // 3)
    ahead = place[0] * span - valid[seq]
    new_keys[...] = keys[...]
    new_values[...] = values[...]

    @pl.when((ahead > -span) & (ahead < prop))
    def _():
        low = low_half(prop)
        early = seq < rows // prop // 2
        key_rows = pl.ds(pl.multiple_of(seq * prop, prop), prop)
        value_rows = pl.ds(pl.multiple_of(rows + seq % (rows // prop // 2) * prop, prop), prop)
        key_tiles, value_tiles = [], []
        for head in range(0, heads, 2):
            one, two = fresh[head, key_rows].astype(f32), fresh[head + 1, key_rows].astype(f32)
            key_tiles.append(turned(jnp.where(low, two, one)))
            one, two = fresh[head, value_rows].astype(f32), fresh[head + 1, value_rows].astype(f32)
            one = jnp.where(early, one, turned(one))
            two = jnp.where(early, turned(two), two)
            value_tiles.append(jnp.where(low, one, two))
        offset = ahead + lax.broadcasted_iota(jnp.int32, (span, prop), 0)
        chooser = jnp.where(offset == lax.broadcasted_iota(jnp.int32, (span, prop), 1), 1.0, 0.0).astype(bf16)
        offset = ahead + lax.broadcasted_iota(jnp.int32, (span, 1), 0)
        inside = (offset >= 0) & (offset < prop)
        for tiles, old, new in ((key_tiles, keys, new_keys), (value_tiles, values, new_values)):
            placed = dot(chooser, jnp.concatenate(tiles, axis=1).astype(bf16))
            new[0] = jnp.where(inside, placed, old[0].astype(f32)).astype(bf16)


VMEM = pl.BlockSpec(memory_space=pltpu.VMEM)
SMEM = pl.BlockSpec(memory_space=pltpu.SMEM)


def call(body, outs, specs, flops, moved, limit):
    return pl.pallas_call(
        body,
        out_shape=outs,
        in_specs=specs,
        out_specs=jax.tree.map(lambda _: VMEM, outs),
        cost_estimate=pl.CostEstimate(flops=flops, bytes_accessed=moved, transcendentals=0),
        compiler_params=pltpu.CompilerParams(vmem_limit_bytes=limit * MIB),
    )


def shape(*dims, dtype=f32):
    return jax.ShapeDtypeStruct(dims, dtype)


def exchanged(slots, axis):
    return lax.all_to_all(slots, axis, 0, 0, tiled=True)


def shards(
    tokens,
    norm_gain,
    w_query,
    w_key,
    w_value,
    query_gain,
    key_gain,
    head_bias,
    w_output,
    cache_keys,
    cache_values,
    base_length,
    accepted,
    parents,
):
    seqs, prop = parents.shape
    heads = head_bias.shape[0]
    rows, span = seqs * prop, cache_keys.shape[1]
    half = rows // 2
    columns = w_output.shape[1]
    peers = lax.axis_size(KV)
    width = tokens.shape[1] * peers
    assert peers == heads and seqs == 4 and rows <= LANES and heads % 4 == 0 and prop == 16
    place = lax.axis_index(KV).astype(jnp.int32).reshape(1)
    valid = base_length + accepted
    parent_column = parents.reshape(rows, 1)
    gains = [jnp.concatenate((g, g)).reshape(1, LANES) for g in (query_gain, key_gain)]

    slots = call(
        project_kernel,
        shape(heads, rows + half + 8, LANES),
        [VMEM] * 5,
        10**8,
        3 * MIB,
        12,
    )(tokens, norm_gain.reshape(1, -1), w_query, w_key, w_value)
    got = exchanged(slots, KV)
    slots, own = call(
        functools.partial(normalize_kernel, width),
        (shape(peers, rows + half, LANES, dtype=bf16), shape(rows + half, LANES, dtype=bf16)),
        [SMEM, VMEM, VMEM, VMEM],
        10**7,
        MIB,
        8,
    )(place, got, *gains)
    fresh = exchanged(slots, KV)
    tree = call(
        functools.partial(tree_kernel, prop),
        shape(2, half, LANES),
        [SMEM, SMEM, VMEM, VMEM],
        10**7,
        MIB // 8,
        8,
    )(place, head_bias, own, parent_column)
    slots = call(
        functools.partial(attend_kernel, prop),
        shape(heads, half + prop, LANES),
        [SMEM, SMEM, SMEM, VMEM, VMEM, VMEM],
        4 * 10**8,
        5 * MIB,
        24,
    )(place, valid, head_bias, fresh, cache_keys, cache_values)
    got = exchanged(slots, KV)
    block = pl.BlockSpec((1, span, cache_keys.shape[2]), lambda s: (s, 0, 0))
    updated_keys, updated_values = pl.pallas_call(
        functools.partial(update_kernel, prop),
        grid=(seqs,),
        out_shape=(cache_keys, cache_values),
        in_specs=[SMEM, SMEM, VMEM, block, block],
        out_specs=(block, block),
        cost_estimate=pl.CostEstimate(flops=10**8, bytes_accessed=8 * MIB, transcendentals=0),
        compiler_params=pltpu.CompilerParams(vmem_limit_bytes=16 * MIB),
    )(place, valid, fresh, cache_keys, cache_values)
    slots = call(combine_kernel, shape(peers, half, LANES, dtype=bf16), [VMEM] * 2, 10**7, MIB, 8)(got, tree)
    got = exchanged(slots, KV)
    part = call(output_kernel, shape(rows, columns), [VMEM] * 2, 10**8, MIB, 8)(got, w_output)
    other = lax.ppermute(part, "tp", [(0, 1), (1, 0)])
    mix, slots = call(
        squares_kernel, (shape(rows, columns), shape(peers, 8, LANES)), [VMEM] * 2, 10**6, MIB // 4, 4
    )(part, other)
    got = exchanged(slots, KV)
    layer_out = call(
        functools.partial(finish_kernel, columns * peers),
        shape(rows, columns, dtype=bf16),
        [VMEM] * 2,
        10**6,
        MIB // 8,
        4,
    )(mix, got)
    return (layer_out, updated_keys, updated_values)


def solution(mesh):
    finer = Mesh(
        mesh.devices.reshape(mesh.shape["dp"], 4, 4, mesh.shape["tp"]), ("dp", "kv_0", "kv_1", "tp")
    )
    return jax.shard_map(
        shards,
        mesh=finer,
        in_specs=(
            P("dp", KV),
            P(KV),
            P(KV, "tp"),
            P(KV, "tp"),
            P(KV, "tp"),
            P(),
            P(),
            P("tp"),
            P("tp", KV),
            P("dp", KV, "tp"),
            P("dp", KV, "tp"),
            P("dp"),
            P("dp"),
            P("dp", None),
        ),
        out_specs=(P("dp", KV), P("dp", KV, "tp"), P("dp", KV, "tp")),
        check_vma=False,
    )
```

time: 189 us -> 89.3 us (0.47)
  blocking collectives: 44.4 us -> 10.9 us
  waiting for transfers between devices: 68.9 us -> 36.7 us
  matrix products: 17.2 us -> 0 us
  between operations: 14.5 us -> 0.82 us
  other arithmetic: 12.3 us -> 0.08 us
  Pallas kernels: 0 us -> 11.2 us
  local copies, waits for them, and re-layouts: 17.2 us -> 9.79 us
  starting transfers between devices: 13.1 us -> 19 us
    all_gather x1 -> x0, waiting for transfers between devices: 57.6 us -> none  [over_pieces(): blocks = lax.all_gather(x, axis)]
    all_to_all x2 -> x4, waiting for transfers between devices: 11.3 us -> 35.4 us  [exchanged(): return lax.all_to_all(slots, axis, 0, 0, tiled=True)]
    all_gather x1 -> x0, blocking collectives: 21.6 us -> none  [sent_together(): lax.all_gather(both, axis, axis=dim, tiled=True)]
    psum x2 -> x0, blocking collectives: 19 us -> none  [by_axis(): return functools.reduce(lax.psum, axes, x)]
    dot_general x26 -> x0, matrix products: 17.2 us -> none  [the longest x2 5.28 us: later_sum(): jnp.einsum('shqp,pr->shqr', values, after, precision=lax.Precision.HIGHEST)]
    pallas_call x0 -> x9, Pallas kernels: none -> 11.2 us  [the longest x1 3.65 us: shards(): call(functools.partial(attend_kernel, prop), shape(heads, half + prop, LA...]
    all_to_all x1, blocking collectives: 3.84 us -> 10.9 us  [exchanged(): return lax.all_to_all(slots, axis, 0, 0, tiled=True)]
    reduce_sum x9 -> x0, other arithmetic: 6.79 us -> none  [the longest x1 4.26 us: over_pieces(): return blocks.sum(axis=0)]
  transfers between devices with their start and end apart: 3 -> 5, of which waited for: 3 -> 5; matrix products, arithmetic and copies ran while one was open for 12% -> 0% of each run, Pallas kernels for 0% -> 5%
where the time goes in v1:
time: 89.3 us; the launch traced here: 88.5 us
  waiting for transfers between devices  36.7 us (41%)
  starting transfers between devices  19 us (21%)
  Pallas kernels  11.2 us (13%)
  blocking collectives  10.9 us (12%)
  local copies, waits for them, and re-layouts  9.79 us (11%)
    all_to_all x4, waiting for transfers between devices, exchanged(): return lax.all_to_all(slots, axis, 0, 0, tiled=True)  35.4 us
    all_to_all x4, starting transfers between devices, exchanged(): return lax.all_to_all(slots, axis, 0, 0, tiled=True)  18.9 us
    all_to_all x1, blocking collectives, exchanged(): return lax.all_to_all(slots, axis, 0, 0, tiled=True)  10.9 us
    unnamed x32, local copies, waits for them, and re-layouts  9.71 us
    pallas_call x1, Pallas kernels, shards(): call(functools.partial(attend_kernel, prop), shape(heads, half + prop, LA...  3.65 us
    pallas_call x1, Pallas kernels, shards(): pl.pallas_call(functools.partial(update_kernel, prop), grid=(seqs,), out_...  2.97 us
  transfers between devices with their start and end apart: 5, of which 5 were waited for; matrix products, arithmetic and copies ran while one was open for 0% of the time, Pallas kernels for 5%

profile of v1, /device:TPU:0, one launch (start us, length us, event | category | flops | bytes accessed | tf_op | source)
XLA Modules:
  0.0 88.5 jit_solution(16958002146360983135)
XLA Ops:
  0.6 0.0 copy-start.13
  0.6 0.0 copy-start.12
  0.7 0.0 copy-start.5
  0.7 1.0 %copy-done.5 = bf16[256,1024]{1,0:T(8,128)(2,1)S(1)} copy-done((bf16[256,1024]{1,0:T(8,128)(2,1)S(1)}, bf16[256,1024]{1,0:T(8,128)(2,1)}, u32[]{:S(2)}) %copy-start.5) | copy-done | bytes 524312
  1.7 0.0 copy-start.6
  1.7 1.0 %copy-done.6 = bf16[256,1024]{1,0:T(8,128)(2,1)S(1)} copy-done((bf16[256,1024]{1,0:T(8,128)(2,1)S(1)}, bf16[256,1024]{1,0:T(8,128)(2,1)}, u32[]{:S(2)}) %copy-start.6) | copy-done | bytes 524312
  2.7 0.0 copy-start.7
  2.8 1.0 %copy-done.7 = bf16[256,1024]{1,0:T(8,128)(2,1)S(1)} copy-done((bf16[256,1024]{1,0:T(8,128)(2,1)S(1)}, bf16[256,1024]{1,0:T(8,128)(2,1)}, u32[]{:S(2)}) %copy-start.7) | copy-done | bytes 524312
  3.8 0.0 copy-start.8
  3.8 0.8 copy-done.8
  4.5 0.0 copy-start.10
  4.6 0.7 copy-done.10
  5.2 0.5 shard_map.157
  5.7 0.0 copy-start.3
  5.7 0.9 %copy-done.3 = f32[16,104,128]{2,1,0:T(8,128)} copy-done((f32[16,104,128]{2,1,0:T(8,128)}, f32[16,104,128]{2,1,0:T(8,128)S(1)}, u32[]{:S(2)}) %copy-start.3) | copy-done | bytes 851992
  6.6 0.0 copy-start.14
  6.6 0.0 copy-start.15
  6.6 0.0 copy-start
  6.6 0.0 copy-start.9
  6.6 8.3 %all-to-all-start = ((f32[16,104,128]{2,1,0:T(8,128)}), f32[16,104,128]{2,1,0:T(8,128)S(1)}, u32[]{:S(2)}, u32[]{:S(2)}) async-start(f32[16,104,128]{2,1,0:T(8,128)} %copy-done.3), calls=%async_computation | async-start | bytes 1703936 | tf_op jit(solution)/shard_map/all_to_all | solution.py:305
  15.0 0.0 copy-done.13
  15.0 0.0 copy-done.12
  15.0 0.1 maximum_bitcast_fusion
  15.1 15.2 %all-to-all-done.got = f32[16,104,128]{2,1,0:T(8,128)S(1)} async-done(((f32[16,104,128]{2,1,0:T(8,128)}), f32[16,104,128]{2,1,0:T(8,128)S(1)}, u32[]{:S(2)}, u32[]{:S(2)}) %all-to-all-start) | async-done | bytes 852000 | tf_op jit(solution)/shard_map/all_to_all | solution.py:305
  30.3 0.9 %shard_map.158 = (bf16[16,96,128]{2,1,0:T(8,128)(2,1)}, bf16[96,128]{1,0:T(8,128)(2,1)S(1)}) custom-call(s32[1]{0:T(128)} %bitcast.place, f32[16,104,128]{2,1,0:T(8,128)S(1)} %all-to-all-done.got, f32[1,128]{1,0:T(1,128)S(1)} %get-tuple-element.15.query_gain, f32[1,128]{1,0:T(1,128)S(1)} %get-tuple-element.16.key_gain), custom_call_target="tpu_custom_call" | custom-call | flops 10000000 | bytes 1048576 | tf_op jit(solution)/shard_map/pallas_call | solution.py:346
  31.2 3.6 %all-to-all-start.1 = ((bf16[16,96,128]{2,1,0:T(8,128)(2,1)}), bf16[16,96,128]{2,1,0:T(8,128)(2,1)S(1)}, u32[]{:S(2)}, u32[]{:S(2)}) async-start(bf16[16,96,128]{2,1,0:T(8,128)(2,1)} %get-tuple-element.9), calls=%async_computation.1 | async-start | bytes 786432 | tf_op jit(solution)/shard_map/all_to_all | solution.py:305
  34.7 0.0 copy-done.14
  34.7 0.0 copy-done.15
  34.8 9.3 %all-to-all-done.1.fresh = bf16[16,96,128]{2,1,0:T(8,128)(2,1)S(1)} async-done(((bf16[16,96,128]{2,1,0:T(8,128)(2,1)}), bf16[16,96,128]{2,1,0:T(8,128)(2,1)S(1)}, u32[]{:S(2)}, u32[]{:S(2)}) %all-to-all-start.1) | async-done | bytes 393248 | tf_op jit(solution)/shard_map/all_to_all | solution.py:305
  44.1 0.0 copy-done
  44.1 0.0 copy-done.9
  44.1 0.0 copy-start.1
  44.1 1.6 %copy-done.1 = bf16[4,256,1024]{2,1,0:T(8,128)(2,1)S(1)} copy-done((bf16[4,256,1024]{2,1,0:T(8,128)(2,1)S(1)}, bf16[4,256,1024]{2,1,0:T(8,128)(2,1)}, u32[]{:S(2)}) %copy-start.1) | copy-done | bytes 2097176
  45.7 0.0 copy-start.11
  45.7 3.7 %shard_map.159 = f32[16,48,128]{2,1,0:T(8,128)} custom-call(s32[1]{0:T(128)} %bitcast.place, s32[4]{0:T(128)S(1)} %add.7.valid, f32[16]{0:T(128)S(1)} %copy-done.9, bf16[16,96,128]{2,1,0:T(8,128)(2,1)S(1)} %all-to-all-done.1.fresh, bf16[4,256,1024]{2,1,0:T(8,128)(2,1)S(1)} %copy-done, bf16[4,256,1024]{2,1,0:T(8,128)(2,1)S(1)} %copy-done.1), custom_call_target="tpu_custom_call" | custom-call | flops 400000000 | bytes 5242880 | tf_op jit(solution)/shard_map/pallas_call | solution.py:363
  49.3 3.6 %all-to-all-start.2 = ((f32[16,48,128]{2,1,0:T(8,128)}), f32[16,48,128]{2,1,0:T(8,128)S(1)}, u32[]{:S(2)}, u32[]{:S(2)}) async-start(f32[16,48,128]{2,1,0:T(8,128)} %shard_map.159), calls=%async_computation.2 | async-start | bytes 786432 | tf_op jit(solution)/shard_map/all_to_all | solution.py:305
  52.9 0.0 copy-done.11
  52.9 0.1 reshape.26.parents
  53.0 1.4 %shard_map.160.tree = f32[2,32,128]{2,1,0:T(8,128)S(1)} custom-call(s32[1]{0:T(128)} %bitcast.place, f32[16]{0:T(128)S(1)} %copy-done.9, bf16[96,128]{1,0:T(8,128)(2,1)S(1)} %get-tuple-element.10.own, s32[64,1]{1,0:T(8,128)S(1)} %reshape.26.parents), custom_call_target="tpu_custom_call" | custom-call | flops 10000000 | bytes 131072 | tf_op jit(solution)/shard_map/pallas_call | solution.py:355
  54.4 7.8 %all-to-all-done.2.got = f32[16,48,128]{2,1,0:T(8,128)S(1)} async-done(((f32[16,48,128]{2,1,0:T(8,128)}), f32[16,48,128]{2,1,0:T(8,128)S(1)}, u32[]{:S(2)}, u32[]{:S(2)}) %all-to-all-start.2) | async-done | bytes 393248 | tf_op jit(solution)/shard_map/all_to_all | solution.py:305
  62.2 0.1 shard_map.161
  62.4 10.9 %all_to_all.25.got = bf16[16,32,128]{2,1,0:T(8,128)(2,1)S(1)} all-to-all(bf16[16,32,128]{2,1,0:T(8,128)(2,1)S(1)} %shard_map.161), channel_id=1, replica_groups=mesh['dp'=4,'kv_0'=4,'kv_1'=4,'tp'=2] {'kv_0','kv_1'}, dimensions={0} | all-to-all | bytes 262144 | tf_op jit(solution)/shard_map/all_to_all | solution.py:305
  73.3 0.0 copy-start.4
  73.3 1.0 %copy-done.4 = bf16[1024,256]{1,0:T(8,128)(2,1)S(1)} copy-done((bf16[1024,256]{1,0:T(8,128)(2,1)S(1)}, bf16[1024,256]{1,0:T(8,128)(2,1)}, u32[]{:S(2)}) %copy-start.4) | copy-done | bytes 524312
  74.3 0.2 shard_map.162.one
  74.6 0.1 collective-permute-start
  74.7 1.2 %collective-permute-done.two = f32[64,256]{1,0:T(8,128)S(1)} collective-permute-done((f32[64,256]{1,0:T(8,128)S(1)}, f32[64,256]{1,0:T(8,128)S(1)}, u32[]{:S(2)}, u32[]{:S(2)}) %collective-permute-start) | collective-permute-done | bytes 65568 | tf_op jit(solution)/shard_map/ppermute | solution.py:385
  75.9 0.7 shard_map.163
  76.6 3.5 %all-to-all-start.4 = ((f32[16,8,128]{2,1,0:T(8,128)}), f32[16,8,128]{2,1,0:T(8,128)S(1)}, u32[]{:S(2)}, u32[]{:S(2)}) async-start(f32[16,8,128]{2,1,0:T(8,128)} %get-tuple-element.12), calls=%async_computation.4 | async-start | bytes 131072 | tf_op jit(solution)/shard_map/all_to_all | solution.py:305
  80.1 0.0 copy-start.2
  80.1 1.6 %copy-done.2 = bf16[4,256,1024]{2,1,0:T(8,128)(2,1)S(1)} copy-done((bf16[4,256,1024]{2,1,0:T(8,128)(2,1)S(1)}, bf16[4,256,1024]{2,1,0:T(8,128)(2,1)}, u32[]{:S(2)}) %copy-start.2) | copy-done | bytes 2097176
  81.7 3.0 %shard_map.165 = (bf16[4,256,1024]{2,1,0:T(8,128)(2,1)}, bf16[4,256,1024]{2,1,0:T(8,128)(2,1)}) custom-call(s32[1]{0:T(128)} %bitcast.place, s32[4]{0:T(128)S(1)} %add.7.valid, bf16[16,96,128]{2,1,0:T(8,128)(2,1)S(1)} %all-to-all-done.1.fresh, bf16[4,256,1024]{2,1,0:T(8,128)(2,1)S(1)} %copy-done, bf16[4,256,1024]{2,1,0:T(8,128)(2,1)S(1)} %copy-done.2), custom_call_target="tpu_custom_call" | custom-call | flops 100000000 | bytes 8388608 | tf_op jit(solution)/shard_map/pallas_call | solution.py:373
  84.7 3.0 %all-to-all-done.4.got = f32[16,8,128]{2,1,0:T(8,128)S(1)} async-done(((f32[16,8,128]{2,1,0:T(8,128)}), f32[16,8,128]{2,1,0:T(8,128)S(1)}, u32[]{:S(2)}, u32[]{:S(2)}) %all-to-all-start.4) | async-done | bytes 65568 | tf_op jit(solution)/shard_map/all_to_all | solution.py:305
  87.7 0.7 shard_map.164
  (1 shorter events, 0.0 us)
Async XLA Ops:
  0.6 14.3 %copy-start.13 = (f32[64]{0:T(128)S(1)}, f32[64]{0:T(128)}, u32[]{:S(2)}) copy-start(f32[64]{0:T(128)} %param.20) | copy-start | bytes 772
  0.6 14.3 %copy-start.12 = (f32[64]{0:T(128)S(1)}, f32[64]{0:T(128)}, u32[]{:S(2)}) copy-start(f32[64]{0:T(128)} %param.19) | copy-start | bytes 772
  0.7 1.1 %copy-start.5 = (bf16[256,1024]{1,0:T(8,128)(2,1)S(1)}, bf16[256,1024]{1,0:T(8,128)(2,1)}, u32[]{:S(2)}) copy-start(bf16[256,1024]{1,0:T(8,128)(2,1)} %w_query.1) | copy-start | bytes 1572868
  1.7 1.0 %copy-start.6 = (bf16[256,1024]{1,0:T(8,128)(2,1)S(1)}, bf16[256,1024]{1,0:T(8,128)(2,1)}, u32[]{:S(2)}) copy-start(bf16[256,1024]{1,0:T(8,128)(2,1)} %w_key.1) | copy-start | bytes 1572868
  2.7 1.0 %copy-start.7 = (bf16[256,1024]{1,0:T(8,128)(2,1)S(1)}, bf16[256,1024]{1,0:T(8,128)(2,1)}, u32[]{:S(2)}) copy-start(bf16[256,1024]{1,0:T(8,128)(2,1)} %w_value.1) | copy-start | bytes 1572868
  3.8 0.8 copy-start.8
  4.5 0.7 copy-start.10
  5.7 0.9 %copy-start.3 = (f32[16,104,128]{2,1,0:T(8,128)}, f32[16,104,128]{2,1,0:T(8,128)S(1)}, u32[]{:S(2)}) copy-start(f32[16,104,128]{2,1,0:T(8,128)S(1)} %shard_map.157) | copy-start | bytes 2555908
  6.6 28.1 %copy-start.14 = (s32[4]{0:T(128)S(1)}, s32[4]{0:T(128)}, u32[]{:S(2)}) copy-start(s32[4]{0:T(128)} %param.25) | copy-start | bytes 52
  6.6 28.1 %copy-start.15 = (s32[4]{0:T(128)S(1)}, s32[4]{0:T(128)}, u32[]{:S(2)}) copy-start(s32[4]{0:T(128)} %param.26) | copy-start | bytes 52
  6.6 37.4 %copy-start = (bf16[4,256,1024]{2,1,0:T(8,128)(2,1)S(1)}, bf16[4,256,1024]{2,1,0:T(8,128)(2,1)}, u32[]{:S(2)}) copy-start(bf16[4,256,1024]{2,1,0:T(8,128)(2,1)} %keys.3) | copy-start | bytes 6291460
  6.6 37.4 %copy-start.9 = (f32[16]{0:T(128)S(1)}, f32[16]{0:T(128)}, u32[]{:S(2)}) copy-start(f32[16]{0:T(128)} %bias.3) | copy-start | bytes 196
  6.6 23.6 %all-to-all-start = ((f32[16,104,128]{2,1,0:T(8,128)}), f32[16,104,128]{2,1,0:T(8,128)S(1)}, u32[]{:S(2)}, u32[]{:S(2)}) async-start(f32[16,104,128]{2,1,0:T(8,128)} %copy-done.3), calls=%async_computation | async-start | bytes 1703936 | tf_op jit(solution)/shard_map/all_to_all | solution.py:305
  31.2 12.9 %all-to-all-start.1 = ((bf16[16,96,128]{2,1,0:T(8,128)(2,1)}), bf16[16,96,128]{2,1,0:T(8,128)(2,1)S(1)}, u32[]{:S(2)}, u32[]{:S(2)}) async-start(bf16[16,96,128]{2,1,0:T(8,128)(2,1)} %get-tuple-element.9), calls=%async_computation.1 | async-start | bytes 786432 | tf_op jit(solution)/shard_map/all_to_all | solution.py:305
  44.1 1.6 %copy-start.1 = (bf16[4,256,1024]{2,1,0:T(8,128)(2,1)S(1)}, bf16[4,256,1024]{2,1,0:T(8,128)(2,1)}, u32[]{:S(2)}) copy-start(bf16[4,256,1024]{2,1,0:T(8,128)(2,1)} %values.3) | copy-start | bytes 6291460
  45.7 7.2 %copy-start.11 = (s32[4,16]{1,0:T(4,128)S(1)}, s32[4,16]{1,0:T(4,128)}, u32[]{:S(2)}) copy-start(s32[4,16]{1,0:T(4,128)} %param.27) | copy-start | bytes 772
  49.3 12.9 %all-to-all-start.2 = ((f32[16,48,128]{2,1,0:T(8,128)}), f32[16,48,128]{2,1,0:T(8,128)S(1)}, u32[]{:S(2)}, u32[]{:S(2)}) async-start(f32[16,48,128]{2,1,0:T(8,128)} %shard_map.159), calls=%async_computation.2 | async-start | bytes 786432 | tf_op jit(solution)/shard_map/all_to_all | solution.py:305
  73.3 1.0 %copy-start.4 = (bf16[1024,256]{1,0:T(8,128)(2,1)S(1)}, bf16[1024,256]{1,0:T(8,128)(2,1)}, u32[]{:S(2)}) copy-start(bf16[1024,256]{1,0:T(8,128)(2,1)} %w_output.1) | copy-start | bytes 1572868
  74.6 1.3 %collective-permute-start = (f32[64,256]{1,0:T(8,128)S(1)}, f32[64,256]{1,0:T(8,128)S(1)}, u32[]{:S(2)}, u32[]{:S(2)}) collective-permute-start(f32[64,256]{1,0:T(8,128)S(1)} %shard_map.162.one), channel_id=1, source_target_pairs={{0,1},{1,0},{2,3},{3,2},{4,5},{5,4},{6,7},{7,6},{8,9},{9,8},{10,11... | collective-permute-start | bytes 196616 | tf_op jit(solution)/shard_map/ppermute | solution.py:385
  76.6 11.1 %all-to-all-start.4 = ((f32[16,8,128]{2,1,0:T(8,128)}), f32[16,8,128]{2,1,0:T(8,128)S(1)}, u32[]{:S(2)}, u32[]{:S(2)}) async-start(f32[16,8,128]{2,1,0:T(8,128)} %get-tuple-element.12), calls=%async_computation.4 | async-start | bytes 131072 | tf_op jit(solution)/shard_map/all_to_all | solution.py:305
  80.1 1.6 %copy-start.2 = (bf16[4,256,1024]{2,1,0:T(8,128)(2,1)S(1)}, bf16[4,256,1024]{2,1,0:T(8,128)(2,1)}, u32[]{:S(2)}) copy-start(bf16[4,256,1024]{2,1,0:T(8,128)(2,1)} %values.3) | copy-start | bytes 6291460

commit v2 on v1

--- a/solution.py
+++ b/solution.py
@@ -48,39 +48,54 @@
     return -jnp.maximum(z, 0.0) - spill, jnp.minimum(z, 0.0) - spill
 
 
-def project_kernel(tokens, gain, w_query, w_key, w_value, slots):
+def project_kernel(*refs):
+    sources, slots, (tokens, gain, w_query, w_key, w_value), arrived = refs[:5], refs[5], refs[6:11], refs[11]
+    copies = [
+        pltpu.make_async_copy(source, held, arrived.at[at])
+        for at, (source, held) in enumerate(zip(sources, refs[6:11]))
+    ]
+    for copy in copies:
+        copy.start()
     rows, half = tokens.shape[0], tokens.shape[0] // 2
+    low, low_v = low_half(rows), low_half(half)
+    copies[0].wait()
     wide = tokens[...].astype(f32)
-    scaled = (wide * gain[...]).astype(bf16)
-    low, low_v = low_half(rows), low_half(half)
-    for at in range(0, w_query.shape[1], 2 * LANES):
-        columns = pl.ds(at, 2 * LANES)
-        query = dot(scaled, w_query[:, columns])
-        key = dot(scaled, w_key[:, columns])
-        value = dot(scaled, w_value[:, columns])
-        for tile in range(2):
-            head = at // HEAD_DIM + 2 * tile
-            lanes = slice(tile * LANES, (tile + 1) * LANES)
-            q, k, v = query[:, lanes], turned(key[:, lanes]), value[:, lanes]
-            v_turned = turned(v)
-            slots[head, :rows] = jnp.where(low, q, k)
-            slots[head + 1, :rows] = jnp.where(low, k, q)
-            slots[head, rows : rows + half] = jnp.where(low_v, v[:half], v_turned[half:])
-            slots[head + 1, rows : rows + half] = jnp.where(low_v, v_turned[:half], v[half:])
     squares = wide * wide
     squares = jnp.concatenate((squares, jnp.zeros((LANES - rows, squares.shape[1]), f32)), axis=0)
     ones = jnp.ones((8, squares.shape[1]), bf16)
     row_squares = sum(dot_nt(ones, part) for part in split_bf16(squares, 3))
     for head in range(slots.shape[0]):
         slots[head, rows + half :] = row_squares
-
-
-def normalize_kernel(width, place, got, query_gain, key_gain, slots, own):
+    copies[1].wait()
+    scaled = (wide * gain[...]).astype(bf16)
+    copies[2].wait()
+    copies[3].wait()
+    spans = [pl.ds(at, 2 * LANES) for at in range(0, w_query.shape[1], 2 * LANES)]
+    tiles = [slice(0, LANES), slice(LANES, 2 * LANES)]
+    for at, columns in enumerate(spans):
+        query, key = dot(scaled, w_query[:, columns]), dot(scaled, w_key[:, columns])
+        for tile, lanes in enumerate(tiles):
+            head = 4 * at + 2 * tile
+            q, k = query[:, lanes], turned(key[:, lanes])
+            slots[head, :rows] = jnp.where(low, q, k)
+            slots[head + 1, :rows] = jnp.where(low, k, q)
+    copies[4].wait()
+    for at, columns in enumerate(spans):
+        value = dot(scaled, w_value[:, columns])
+        for tile, lanes in enumerate(tiles):
+            head = 4 * at + 2 * tile
+            v = value[:, lanes]
+            v_turned = turned(v)
+            slots[head, rows : rows + half] = jnp.where(low_v, v[:half], v_turned[half:])
+            slots[head + 1, rows : rows + half] = jnp.where(low_v, v_turned[:half], v[half:])
+
+
+def normalize_kernel(width, got, query_gain, key_gain, slots, own):
     peers = got.shape[0]
     rows = got.shape[1] - 8
     half = rows // 3
     rows = 2 * half
-    even = place[0] % 2 == 0
+    even = lax.axis_index(KV) % 2 == 0
     total = got[0]
     for peer in range(1, peers):
         total = total + got[peer]
@@ -90,9 +105,9 @@
     low_sum = jnp.sum(jnp.where(low, power, 0.0), axis=1, keepdims=True)
     high_sum = jnp.sum(jnp.where(low, 0.0, power), axis=1, keepdims=True)
     factor = lax.rsqrt(jnp.where(low, low_sum, high_sum) / HEAD_DIM + epsilon)
-    low_gain = jnp.where(even, query_gain[...], key_gain[...])
-    high_gain = jnp.where(even, key_gain[...], query_gain[...])
-    normed = (both * factor * jnp.where(low, low_gain, high_gain)).astype(bf16)
+    one, two = query_gain[...], key_gain[...]
+    gain = jnp.concatenate((jnp.where(even, one, two), jnp.where(even, two, one)), axis=1)
+    normed = (both * factor * gain).astype(bf16)
     inv_rms = jnp.broadcast_to(lax.rsqrt(squares / width + epsilon), (half, LANES))
     lane = lax.broadcasted_iota(jnp.int32, (half, LANES), 1)
     row = lax.broadcasted_iota(jnp.int32, (half, LANES), 0)
@@ -106,19 +121,26 @@
         slots[peer, rows:] = fresh
 
 
-def tree_kernel(prop, place, bias, own, parents, out):
+def tree_part(prop, bias, own, parents, out):
     half = own.shape[0] // 3
     rows = 2 * half
-    even = place[0] % 2 == 0
+    even = lax.axis_index(KV) % 2 == 0
     low = low_half(rows)
     both = own[:rows].astype(f32)
     other = turned(both)
     query = jnp.where(low, jnp.where(even, both, other), 0.0).astype(bf16)
     key = jnp.where(even, other, both).astype(bf16)
-    score = dot_nt(query, key) * HEAD_DIM ** (-0.5) + bias[place[0]]
+    score = dot_nt(query, key) * HEAD_DIM ** (-0.5) + bias[lax.axis_index(KV)]
     row = lax.broadcasted_iota(jnp.int32, (rows, rows), 0)
     column = lax.broadcasted_iota(jnp.int32, (rows, rows), 1)
-    parent = parents[...]
+    small = [lax.broadcasted_iota(jnp.int32, (prop, prop), axis) for axis in range(2)]
+    parent = jnp.concatenate(
+        [
+            jnp.sum(jnp.where(small[0] == small[1], parents[seq : seq + 1], 0), axis=1, keepdims=True)
+            for seq in range(rows // prop)
+        ],
+        axis=0,
+    )
     direct = (parent >= 0) & (column == row - row % prop + parent)
     step = jnp.where(direct, 1.0, 0.0).astype(bf16)
     above = jnp.where(row == column, 1.0, 0.0)
@@ -143,7 +165,7 @@
     out[1] = jnp.where(low, kept[:half], kept[half:])
 
 
-def attend_kernel(prop, place, valid, bias, fresh, keys, values, slots):
+def attend_kernel(prop, base, accepted, bias, fresh, keys, values, slots):
     seqs, span, _ = keys.shape
     heads = fresh.shape[0]
     rows = seqs * prop
@@ -155,11 +177,11 @@
     blank = jnp.zeros((prop, LANES), bf16)
     order = lax.broadcasted_iota(jnp.int32, (span, span), 0)
     after = jnp.where(order > lax.broadcasted_iota(jnp.int32, (span, span), 1), 1.0, 0.0).astype(bf16)
-    position = place[0] * span + lax.broadcasted_iota(jnp.int32, (1, span), 1)
+    position = lax.axis_index(KV) * span + lax.broadcasted_iota(jnp.int32, (1, span), 1)
     quarter = lax.broadcasted_iota(jnp.int32, (prop, LANES), 1) // (LANES // seqs)
     sums, logs = [], []
     for seq in range(seqs):
-        live = position < valid[seq]
+        live = position < base[seq] + accepted[seq]
         scores = []
         for first in range(0, heads, group):
             blocks = []
@@ -250,12 +272,13 @@
     out[...] = (mix[...] * factor).astype(bf16)
 
 
-def update_kernel(prop, place, valid, fresh, keys, values, new_keys, new_values):
+def side_kernel(prop, base, accepted, bias, own, parents, fresh, keys, values, tree, new_keys, new_values):
     seq = pl.program_id(0)
     _, span, _ = keys.shape
     heads = fresh.shape[0]
     rows = 2 * (fresh.shape[1] // 3)
-    ahead = place[0] * span - valid[seq]
+    ahead = lax.axis_index(KV) * span - base[seq] - accepted[seq]
+    pl.when(seq == 0)(functools.partial(tree_part, prop, bias, own, parents, tree))
     new_keys[...] = keys[...]
     new_values[...] = values[...]
 
@@ -329,37 +352,27 @@
     peers = lax.axis_size(KV)
     width = tokens.shape[1] * peers
     assert peers == heads and seqs == 4 and rows <= LANES and heads % 4 == 0 and prop == 16
-    place = lax.axis_index(KV).astype(jnp.int32).reshape(1)
-    valid = base_length + accepted
-    parent_column = parents.reshape(rows, 1)
-    gains = [jnp.concatenate((g, g)).reshape(1, LANES) for g in (query_gain, key_gain)]
-
-    slots = call(
+
+    sources = (tokens, norm_gain.reshape(1, -1), w_query, w_key, w_value)
+    slots = pl.pallas_call(
         project_kernel,
-        shape(heads, rows + half + 8, LANES),
-        [VMEM] * 5,
-        10**8,
-        3 * MIB,
-        12,
-    )(tokens, norm_gain.reshape(1, -1), w_query, w_key, w_value)
+        out_shape=shape(heads, rows + half + 8, LANES),
+        in_specs=[pl.BlockSpec(memory_space=pltpu.HBM)] * 5,
+        out_specs=VMEM,
+        scratch_shapes=[pltpu.VMEM(a.shape, a.dtype) for a in sources] + [pltpu.SemaphoreType.DMA((5,))],
+        cost_estimate=pl.CostEstimate(flops=10**8, bytes_accessed=3 * MIB, transcendentals=0),
+        compiler_params=pltpu.CompilerParams(vmem_limit_bytes=67_000_000),
+    )(*sources)
     got = exchanged(slots, KV)
     slots, own = call(
         functools.partial(normalize_kernel, width),
         (shape(peers, rows + half, LANES, dtype=bf16), shape(rows + half, LANES, dtype=bf16)),
-        [SMEM, VMEM, VMEM, VMEM],
-        10**7,
+        [VMEM, VMEM, VMEM],
+        10**10,
         MIB,
         8,
-    )(place, got, *gains)
+    )(got, query_gain.reshape(1, -1), key_gain.reshape(1, -1))
     fresh = exchanged(slots, KV)
-    tree = call(
-        functools.partial(tree_kernel, prop),
-        shape(2, half, LANES),
-        [SMEM, SMEM, VMEM, VMEM],
-        10**7,
-        MIB // 8,
-        8,
-    )(place, head_bias, own, parent_column)
     slots = call(
         functools.partial(attend_kernel, prop),
         shape(heads, half + prop, LANES),
@@ -367,18 +380,18 @@
         4 * 10**8,
         5 * MIB,
         24,
-    )(place, valid, head_bias, fresh, cache_keys, cache_values)
+    )(base_length, accepted, head_bias, fresh, cache_keys, cache_values)
     got = exchanged(slots, KV)
     block = pl.BlockSpec((1, span, cache_keys.shape[2]), lambda s: (s, 0, 0))
-    updated_keys, updated_values = pl.pallas_call(
-        functools.partial(update_kernel, prop),
+    tree, updated_keys, updated_values = pl.pallas_call(
+        functools.partial(side_kernel, prop),
         grid=(seqs,),
-        out_shape=(cache_keys, cache_values),
-        in_specs=[SMEM, SMEM, VMEM, block, block],
-        out_specs=(block, block),
+        out_shape=(shape(2, half, LANES), cache_keys, cache_values),
+        in_specs=[SMEM, SMEM, SMEM, VMEM, VMEM, VMEM, block, block],
+        out_specs=(VMEM, block, block),
         cost_estimate=pl.CostEstimate(flops=10**8, bytes_accessed=8 * MIB, transcendentals=0),
         compiler_params=pltpu.CompilerParams(vmem_limit_bytes=16 * MIB),
-    )(place, valid, fresh, cache_keys, cache_values)
+    )(base_length, accepted, head_bias, own, parents, fresh, cache_keys, cache_values)
     slots = call(combine_kernel, shape(peers, half, LANES, dtype=bf16), [VMEM] * 2, 10**7, MIB, 8)(got, tree)
     got = exchanged(slots, KV)
     part = call(output_kernel, shape(rows, columns), [VMEM] * 2, 10**8, MIB, 8)(got, w_output)

time: 89.3 us -> 81.3 us (0.910)
  blocking collectives: 10.9 us -> 57.8 us
  waiting for transfers between devices: 36.7 us -> 4.97 us
  starting transfers between devices: 19 us -> 3.64 us
  local copies, waits for them, and re-layouts: 9.79 us -> 1.63 us
    all_to_all x1 -> x4, blocking collectives: 10.9 us -> 57.8 us  [exchanged(): return lax.all_to_all(slots, axis, 0, 0, tiled=True)]
    all_to_all x4 -> x1, waiting for transfers between devices: 35.4 us -> 3.73 us  [exchanged(): return lax.all_to_all(slots, axis, 0, 0, tiled=True)]
    all_to_all x4 -> x1, starting transfers between devices: 18.9 us -> 3.55 us  [exchanged(): return lax.all_to_all(slots, axis, 0, 0, tiled=True)]
    unnamed x32 -> x20, local copies, waits for them, and re-layouts: 9.71 us -> 1.63 us
    pallas_call x3 -> x2, Pallas kernels: 4.86 us -> 6.85 us  [the longest x1 4.02 us: shards(): pl.pallas_call(functools.partial(side_kernel, prop), grid=(seqs,), out_sh...]
  transfers between devices with their start and end apart: 5 -> 2, of which waited for: 5 -> 2; matrix products, arithmetic and copies ran while one was open for 0% -> 0% of each run, Pallas kernels for 5% -> 5%
where the time goes in v2:
time: 81.3 us; the launch traced here: 80.7 us
  blocking collectives  57.8 us (71%)
  Pallas kernels  11.9 us (15%)
  waiting for transfers between devices  4.97 us (6%)
  starting transfers between devices  3.64 us (4%)
  local copies, waits for them, and re-layouts  1.63 us (2%)
    all_to_all x4, blocking collectives, exchanged(): return lax.all_to_all(slots, axis, 0, 0, tiled=True)  57.8 us
    pallas_call x1, Pallas kernels, shards(): pl.pallas_call(functools.partial(side_kernel, prop), grid=(seqs,), out_sh...  4.02 us
    all_to_all x1, waiting for transfers between devices, exchanged(): return lax.all_to_all(slots, axis, 0, 0, tiled=True)  3.73 us
    pallas_call x1, Pallas kernels, shards(): call(functools.partial(attend_kernel, prop), shape(heads, half + prop, LA...  3.66 us
    all_to_all x1, starting transfers between devices, exchanged(): return lax.all_to_all(slots, axis, 0, 0, tiled=True)  3.55 us
    pallas_call x1, Pallas kernels, shards(): pl.pallas_call(project_kernel, out_shape=shape(heads, rows + half + 8, LA...  2.83 us
    unnamed x20, local copies, waits for them, and re-layouts  1.63 us
  transfers between devices with their start and end apart: 2, of which 2 were waited for; matrix products, arithmetic and copies ran while one was open for 0% of the time, Pallas kernels for 5%

profile of v2, /device:TPU:0, one launch (start us, length us, event | category | flops | bytes accessed | tf_op | source)
XLA Modules:
  0.0 80.7 jit_solution(467923727899556647)
XLA Ops:
  0.6 0.0 copy-start.8
  0.6 0.0 copy-start.9
  0.7 2.8 %shard_map.157 = f32[16,104,128]{2,1,0:T(8,128)} custom-call(bf16[64,256]{1,0:T(8,128)(2,1)} %refs_0_.1, f32[1,256]{1,0:T(1,128)} %bitcast.5, bf16[256,1024]{1,0:T(8,128)(2,1)} %refs_2_.1, bf16[256,1024]{1,0:T(8,128)(2,1)} %refs_3_.1, bf16[256,1024]{1,0:T(8,128)(2,1)} %refs_4_.1), custom_call_target="tpu_custom_call" | custom-call | flops 100000000 | bytes 3145728 | tf_op jit(solution)/shard_map/pallas_call | solution.py:357
  3.5 23.2 %all_to_all.25.got = f32[16,104,128]{2,1,0:T(8,128)S(1)} all-to-all(f32[16,104,128]{2,1,0:T(8,128)} %shard_map.157), channel_id=1, replica_groups=mesh['dp'=4,'kv_0'=4,'kv_1'=4,'tp'=2] {'kv_0','kv_1'}, dimensions={0} | all-to-all | bytes 1703936 | tf_op jit(solution)/shard_map/all_to_all | solution.py:328
  26.7 0.0 copy-done.8
  26.7 0.0 copy-done.9
  26.7 0.0 copy-start
  26.7 0.0 copy-start.1
  26.7 0.0 copy-start.5
  26.7 0.0 copy-start.6
  26.7 0.0 copy-start.7
  26.8 0.2 shard_map.158
  26.9 12.6 %all_to_all.26.fresh = bf16[16,96,128]{2,1,0:T(8,128)(2,1)S(1)} all-to-all(bf16[16,96,128]{2,1,0:T(8,128)(2,1)S(1)} %get-tuple-element.10), channel_id=1, replica_groups=mesh['dp'=4,'kv_0'=4,'kv_1'=4,'tp'=2] {'kv_0','kv_1'}, dimensions={0} | all-to-all | bytes 786432 | tf_op jit(solution)/shard_map/all_to_all | solution.py:328
  39.5 0.0 copy-done
  39.5 0.0 copy-done.1
  39.5 0.0 copy-done.5
  39.5 0.0 copy-done.6
  39.6 0.0 copy-done.7
  39.6 0.0 copy-start.4
  39.6 3.7 %shard_map.159 = f32[16,48,128]{2,1,0:T(8,128)} custom-call(s32[4]{0:T(128)S(1)} %copy-done.5, s32[4]{0:T(128)S(1)} %copy-done.6, f32[16]{0:T(128)S(1)} %copy-done.7, bf16[16,96,128]{2,1,0:T(8,128)(2,1)S(1)} %all_to_all.26.fresh, bf16[4,256,1024]{2,1,0:T(8,128)(2,1)S(1)} %copy-done, bf16[4,256,1024]{2,1,0:T(8,128)(2,1)S(1)} %copy-done.1), custom_call_target="tpu_custom_call" | custom-call | flops 400000000 | bytes 5242880 | tf_op jit(solution)/shard_map/pallas_call | solution.py:376
  43.2 3.6 %all-to-all-start.2 = ((f32[16,48,128]{2,1,0:T(8,128)}), f32[16,48,128]{2,1,0:T(8,128)S(1)}, u32[]{:S(2)}, u32[]{:S(2)}) async-start(f32[16,48,128]{2,1,0:T(8,128)} %shard_map.159), calls=%async_computation.2 | async-start | bytes 786432 | tf_op jit(solution)/shard_map/all_to_all | solution.py:328
  46.8 0.0 copy-done.4
  46.8 0.0 copy-start.2
  46.8 1.6 %copy-done.2 = bf16[4,256,1024]{2,1,0:T(8,128)(2,1)S(1)} copy-done((bf16[4,256,1024]{2,1,0:T(8,128)(2,1)S(1)}, bf16[4,256,1024]{2,1,0:T(8,128)(2,1)}, u32[]{:S(2)}) %copy-start.2) | copy-done | bytes 2097176
  48.4 0.0 copy-start.3
  48.4 4.0 %shard_map.160 = (f32[2,32,128]{2,1,0:T(8,128)S(1)}, bf16[4,256,1024]{2,1,0:T(8,128)(2,1)}, bf16[4,256,1024]{2,1,0:T(8,128)(2,1)}) custom-call(s32[4]{0:T(128)S(1)} %copy-done.5, s32[4]{0:T(128)S(1)} %copy-done.6, f32[16]{0:T(128)S(1)} %copy-done.7, bf16[96,128]{1,0:T(8,128)(2,1)S(1)} %get-tuple-element.11.own, s32[4,16]{1,0:T(4,128)S(1)} %copy-done.4, ...), custom_call_target="tpu_custom_call" | custom-call | flops 100000000 | bytes 8388608 | tf_op jit(solution)/shard_map/pallas_call | solution.py:386
  52.4 3.7 %all-to-all-done.2.got = f32[16,48,128]{2,1,0:T(8,128)S(1)} async-done(((f32[16,48,128]{2,1,0:T(8,128)}), f32[16,48,128]{2,1,0:T(8,128)S(1)}, u32[]{:S(2)}, u32[]{:S(2)}) %all-to-all-start.2) | async-done | bytes 393248 | tf_op jit(solution)/shard_map/all_to_all | solution.py:328
  56.2 0.1 shard_map.161
  56.3 11.2 %all_to_all.27.got = bf16[16,32,128]{2,1,0:T(8,128)(2,1)S(1)} all-to-all(bf16[16,32,128]{2,1,0:T(8,128)(2,1)S(1)} %shard_map.161), channel_id=1, replica_groups=mesh['dp'=4,'kv_0'=4,'kv_1'=4,'tp'=2] {'kv_0','kv_1'}, dimensions={0} | all-to-all | bytes 262144 | tf_op jit(solution)/shard_map/all_to_all | solution.py:328
  67.5 0.0 copy-done.3
  67.5 0.3 shard_map.162.one
  67.8 0.1 collective-permute-start
  67.9 1.2 %collective-permute-done.two = f32[64,256]{1,0:T(8,128)S(1)} collective-permute-done((f32[64,256]{1,0:T(8,128)S(1)}, f32[64,256]{1,0:T(8,128)S(1)}, u32[]{:S(2)}, u32[]{:S(2)}) %collective-permute-start) | collective-permute-done | bytes 65568 | tf_op jit(solution)/shard_map/ppermute | solution.py:398
  69.1 0.1 shard_map.163
  69.2 10.7 %all_to_all.28.got = f32[16,8,128]{2,1,0:T(8,128)S(1)} all-to-all(f32[16,8,128]{2,1,0:T(8,128)S(1)} %get-tuple-element.14), channel_id=1, replica_groups=mesh['dp'=4,'kv_0'=4,'kv_1'=4,'tp'=2] {'kv_0','kv_1'}, dimensions={0} | all-to-all | bytes 131072 | tf_op jit(solution)/shard_map/all_to_all | solution.py:328
  80.0 0.7 shard_map.164
Async XLA Ops:
  0.6 26.1 %copy-start.8 = (f32[64]{0:T(128)S(1)}, f32[64]{0:T(128)}, u32[]{:S(2)}) copy-start(f32[64]{0:T(128)} %param.19) | copy-start | bytes 772
  0.6 26.1 %copy-start.9 = (f32[64]{0:T(128)S(1)}, f32[64]{0:T(128)}, u32[]{:S(2)}) copy-start(f32[64]{0:T(128)} %param.20) | copy-start | bytes 772
  26.7 12.8 %copy-start = (bf16[4,256,1024]{2,1,0:T(8,128)(2,1)S(1)}, bf16[4,256,1024]{2,1,0:T(8,128)(2,1)}, u32[]{:S(2)}) copy-start(bf16[4,256,1024]{2,1,0:T(8,128)(2,1)} %keys.3) | copy-start | bytes 6291460
  26.7 12.8 %copy-start.1 = (bf16[4,256,1024]{2,1,0:T(8,128)(2,1)S(1)}, bf16[4,256,1024]{2,1,0:T(8,128)(2,1)}, u32[]{:S(2)}) copy-start(bf16[4,256,1024]{2,1,0:T(8,128)(2,1)} %values.3) | copy-start | bytes 6291460
  26.7 12.8 %copy-start.5 = (s32[4]{0:T(128)S(1)}, s32[4]{0:T(128)}, u32[]{:S(2)}) copy-start(s32[4]{0:T(128)} %base.3) | copy-start | bytes 52
  26.7 12.8 %copy-start.6 = (s32[4]{0:T(128)S(1)}, s32[4]{0:T(128)}, u32[]{:S(2)}) copy-start(s32[4]{0:T(128)} %accepted.3) | copy-start | bytes 52
  26.7 12.8 %copy-start.7 = (f32[16]{0:T(128)S(1)}, f32[16]{0:T(128)}, u32[]{:S(2)}) copy-start(f32[16]{0:T(128)} %bias.3) | copy-start | bytes 196
  39.6 7.2 %copy-start.4 = (s32[4,16]{1,0:T(4,128)S(1)}, s32[4,16]{1,0:T(4,128)}, u32[]{:S(2)}) copy-start(s32[4,16]{1,0:T(4,128)} %parents.1) | copy-start | bytes 772
  43.2 12.9 %all-to-all-start.2 = ((f32[16,48,128]{2,1,0:T(8,128)}), f32[16,48,128]{2,1,0:T(8,128)S(1)}, u32[]{:S(2)}, u32[]{:S(2)}) async-start(f32[16,48,128]{2,1,0:T(8,128)} %shard_map.159), calls=%async_computation.2 | async-start | bytes 786432 | tf_op jit(solution)/shard_map/all_to_all | solution.py:328
  46.8 1.6 %copy-start.2 = (bf16[4,256,1024]{2,1,0:T(8,128)(2,1)S(1)}, bf16[4,256,1024]{2,1,0:T(8,128)(2,1)}, u32[]{:S(2)}) copy-start(bf16[4,256,1024]{2,1,0:T(8,128)(2,1)} %values.3) | copy-start | bytes 6291460
  48.4 19.1 %copy-start.3 = (bf16[1024,256]{1,0:T(8,128)(2,1)S(1)}, bf16[1024,256]{1,0:T(8,128)(2,1)}, u32[]{:S(2)}) copy-start(bf16[1024,256]{1,0:T(8,128)(2,1)} %w_output.1) | copy-start | bytes 1572868
  67.8 1.3 %collective-permute-start = (f32[64,256]{1,0:T(8,128)S(1)}, f32[64,256]{1,0:T(8,128)S(1)}, u32[]{:S(2)}, u32[]{:S(2)}) collective-permute-start(f32[64,256]{1,0:T(8,128)S(1)} %shard_map.162.one), channel_id=1, source_target_pairs={{0,1},{1,0},{2,3},{3,2},{4,5},{5,4},{6,7},{7,6},{8,9},{9,8},{10,11... | collective-permute-start | bytes 196616 | tf_op jit(solution)/shard_map/ppermute | solution.py:398

commit v3 on v2

--- a/solution.py
+++ b/solution.py
@@ -12,6 +12,8 @@
 LANES = 128
 KV = ("kv_0", "kv_1")
 MIB = 1 << 20
+LOG2_E = 1.4426950408889634
+HIDDEN = -1e30
 
 epsilon = 1e-05
 f32 = jnp.float32
@@ -46,6 +48,12 @@
 def signs(z):
     spill = jnp.log(1.0 + jnp.exp(-jnp.abs(z)))
     return -jnp.maximum(z, 0.0) - spill, jnp.minimum(z, 0.0) - spill
+
+
+def exits(z):
+    below, above = jnp.minimum(z, 0.0), jnp.maximum(z, 0.0)
+    spill = jnp.log2(1.0 + jnp.exp2(below - above))
+    return above + spill, below - spill
 
 
 def project_kernel(*refs):
@@ -165,12 +173,12 @@
     out[1] = jnp.where(low, kept[:half], kept[half:])
 
 
-def attend_kernel(prop, base, accepted, bias, fresh, keys, values, slots):
+def attend_kernel(prop, base, accepted, bias, fresh, keys, values, slots, held, sent):
     seqs, span, _ = keys.shape
     heads = fresh.shape[0]
-    rows = seqs * prop
+    half = seqs * prop // 2
     group = 4
-    tall = heads * prop
+    groups = heads // group
     low = low_half(prop)
     low_mask = low.astype(f32).astype(bf16)
     high_mask = (1.0 - low.astype(f32)).astype(bf16)
@@ -178,12 +186,13 @@
     order = lax.broadcasted_iota(jnp.int32, (span, span), 0)
     after = jnp.where(order > lax.broadcasted_iota(jnp.int32, (span, span), 1), 1.0, 0.0).astype(bf16)
     position = lax.axis_index(KV) * span + lax.broadcasted_iota(jnp.int32, (1, span), 1)
+    hidden = [jnp.where(position < base[seq] + accepted[seq], 0.0, HIDDEN) for seq in range(seqs)]
     quarter = lax.broadcasted_iota(jnp.int32, (prop, LANES), 1) // (LANES // seqs)
-    sums, logs = [], []
-    for seq in range(seqs):
-        live = position < base[seq] + accepted[seq]
-        scores = []
-        for first in range(0, heads, group):
+    sending = []
+
+    def scored(at):
+        first, scores = at * group, []
+        for seq in range(seqs):
             blocks = []
             for j in range(group):
                 tile = fresh[first + j, seq * prop : (seq + 1) * prop] * (low_mask if j % 2 == 0 else high_mask)
@@ -192,30 +201,50 @@
             score = dot_nt(jnp.concatenate(blocks, axis=0), stored)
             for j in range(group):
                 part = score[j * prop : (j + 1) * prop]
-                scores.append(part * HEAD_DIM ** (-0.5) + bias[first + j])
-        stay, taken = signs(jnp.concatenate(scores, axis=0))
-        stay = jnp.where(live, stay, 0.0)
-        tail = dot(jnp.concatenate(split_bf16(stay, 2), axis=0), after)
+                scores.append(part * (HEAD_DIM ** (-0.5) * LOG2_E) + (bias[first + j] * LOG2_E + hidden[seq]))
+        return jnp.concatenate(scores, axis=0)
+
+    def suffixes(score):
+        leave, taken = exits(score)
+        tall = leave.shape[0]
+        tail = dot(jnp.concatenate(split_bf16(leave, 2), axis=0), after)
         tail = tail[:tall] + tail[tall:]
-        weight = jnp.where(live, jnp.exp(taken + tail), 0.0).astype(bf16)
-        logs.append(tail[:, :1] + stay[:, :1])
-        tiles = []
-        for first in range(0, heads, group):
+        log = tail[:, :1] + leave[:, :1]
+        return jnp.exp2(taken - tail).astype(bf16), log
+
+    def send(at, weight, log):
+        first, tiles = at * group, []
+        for seq in range(seqs):
             stored = values[seq, :, first * HEAD_DIM : (first + group) * HEAD_DIM]
-            summed = dot(weight[first * prop : (first + group) * prop], stored)
-            for j in range(group):
-                lanes = slice(j // 2 * LANES, (j // 2 + 1) * LANES)
-                tiles.append(summed[j * prop : (j + 1) * prop, lanes])
-        sums.append(tiles)
-    for head in range(heads):
-        for seq in range(seqs // 2):
-            one, two = sums[seq][head], sums[seq + seqs // 2][head]
-            one, two = (one, turned(two)) if head % 2 == 0 else (turned(one), two)
-            slots[head, seq * prop : (seq + 1) * prop] = jnp.where(low, one, two)
-        log = jnp.zeros((prop, LANES), f32)
-        for seq in range(seqs):
-            log = jnp.where(quarter == seq, logs[seq][head * prop : (head + 1) * prop], log)
-        slots[head, rows // 2 :] = log
+            tiles.append(dot(weight[seq * group * prop : (seq + 1) * group * prop], stored))
+        for j in range(group):
+            head = first + j
+            rows = slice(j * prop, (j + 1) * prop)
+            lanes = slice(j // 2 * LANES, (j // 2 + 1) * LANES)
+            for seq in range(seqs // 2):
+                one, two = tiles[seq][rows, lanes], tiles[seq + seqs // 2][rows, lanes]
+                one, two = (one, turned(two)) if j % 2 == 0 else (turned(one), two)
+                held[head, seq * prop : (seq + 1) * prop] = jnp.where(low, one, two)
+            logs = jnp.zeros((prop, LANES), f32)
+            for seq in range(seqs):
+                start = (seq * group + j) * prop
+                logs = jnp.where(quarter == seq, log[start : start + prop], logs)
+            held[head, half:] = logs
+        chosen = pl.ds(first, group)
+        copy = pltpu.make_async_copy(held.at[chosen], slots.at[chosen], sent.at[at])
+        copy.start()
+        sending.append(copy)
+
+    score, ready = scored(0), None
+    for at in range(groups):
+        following = scored(at + 1) if at + 1 < groups else None
+        weight, log = suffixes(score)
+        if ready is not None:
+            send(at - 1, *ready)
+        ready, score = (weight, log), following
+    send(groups - 1, *ready)
+    for copy in sending:
+        copy.wait()
 
 
 def combine_kernel(got, tree, slots):
@@ -227,7 +256,7 @@
     later = jnp.zeros((prop, LANES), f32)
     part = jnp.zeros((half, LANES), f32)
     for block in range(blocks - 1, -1, -1):
-        kept = jnp.exp(later)
+        kept = jnp.exp2(-later)
         one = jnp.where(first, kept, pltpu.roll(kept, HEAD_DIM // 2, 1))
         two = jnp.where(first, pltpu.roll(kept, LANES - HEAD_DIM // 2, 1), kept)
         part = part + jnp.concatenate((one, two), axis=0) * got[block, :half]
@@ -272,37 +301,49 @@
     out[...] = (mix[...] * factor).astype(bf16)
 
 
-def side_kernel(prop, base, accepted, bias, own, parents, fresh, keys, values, tree, new_keys, new_values):
-    seq = pl.program_id(0)
-    _, span, _ = keys.shape
+def side_kernel(
+    prop, base, accepted, bias, own, parents, fresh, keys, values, tree, new_keys, new_values, held, moved
+):
+    seqs, span, _ = keys.shape
     heads = fresh.shape[0]
-    rows = 2 * (fresh.shape[1] // 3)
-    ahead = lax.axis_index(KV) * span - base[seq] - accepted[seq]
-    pl.when(seq == 0)(functools.partial(tree_part, prop, bias, own, parents, tree))
-    new_keys[...] = keys[...]
-    new_values[...] = values[...]
-
-    @pl.when((ahead > -span) & (ahead < prop))
-    def _():
-        low = low_half(prop)
-        early = seq < rows // prop // 2
-        key_rows = pl.ds(pl.multiple_of(seq * prop, prop), prop)
-        value_rows = pl.ds(pl.multiple_of(rows + seq % (rows // prop // 2) * prop, prop), prop)
+    rows = seqs * prop
+    window = 2 * prop
+    loads, stores = [], []
+    for seq in range(seqs):
+        for which, (source, target) in enumerate(((keys, new_keys), (values, new_values))):
+            block = held.at[which, seq]
+            loads.append(pltpu.make_async_copy(source.at[seq], block, moved.at[0, which, seq]))
+            stores.append(pltpu.make_async_copy(block, target.at[seq], moved.at[1, which, seq]))
+    for copy in loads:
+        copy.start()
+    tree_part(prop, bias, own, parents, tree)
+    low = low_half(prop)
+    for seq in range(seqs):
+        start = base[seq] + accepted[seq] - lax.axis_index(KV) * span
+        at = jnp.minimum(jnp.maximum(start, 0), span - window) // prop * prop
+        lines = pl.ds(pl.multiple_of(at, prop), window)
+        start = start - at
+        early = seq < seqs // 2
+        key_rows = slice(seq * prop, (seq + 1) * prop)
+        value_rows = slice(rows + seq % (seqs // 2) * prop, rows + (seq % (seqs // 2) + 1) * prop)
         key_tiles, value_tiles = [], []
         for head in range(0, heads, 2):
             one, two = fresh[head, key_rows].astype(f32), fresh[head + 1, key_rows].astype(f32)
             key_tiles.append(turned(jnp.where(low, two, one)))
             one, two = fresh[head, value_rows].astype(f32), fresh[head + 1, value_rows].astype(f32)
-            one = jnp.where(early, one, turned(one))
-            two = jnp.where(early, turned(two), two)
-            value_tiles.append(jnp.where(low, one, two))
-        offset = ahead + lax.broadcasted_iota(jnp.int32, (span, prop), 0)
-        chooser = jnp.where(offset == lax.broadcasted_iota(jnp.int32, (span, prop), 1), 1.0, 0.0).astype(bf16)
-        offset = ahead + lax.broadcasted_iota(jnp.int32, (span, 1), 0)
+            value_tiles.append(jnp.where(low, one, turned(two)) if early else jnp.where(low, turned(one), two))
+        offset = lax.broadcasted_iota(jnp.int32, (window, prop), 0) - start
+        chooser = jnp.where(offset == lax.broadcasted_iota(jnp.int32, (window, prop), 1), 1.0, 0.0).astype(bf16)
+        offset = lax.broadcasted_iota(jnp.int32, (window, 1), 0) - start
         inside = (offset >= 0) & (offset < prop)
-        for tiles, old, new in ((key_tiles, keys, new_keys), (value_tiles, values, new_values)):
+        for which, tiles in enumerate((key_tiles, value_tiles)):
             placed = dot(chooser, jnp.concatenate(tiles, axis=1).astype(bf16))
-            new[0] = jnp.where(inside, placed, old[0].astype(f32)).astype(bf16)
+            loads[2 * seq + which].wait()
+            old = held[which, seq, lines].astype(f32)
+            held[which, seq, lines] = jnp.where(inside, placed, old).astype(bf16)
+            stores[2 * seq + which].start()
+    for copy in stores:
+        copy.wait()
 
 
 VMEM = pl.BlockSpec(memory_space=pltpu.VMEM)
@@ -353,15 +394,19 @@
     width = tokens.shape[1] * peers
     assert peers == heads and seqs == 4 and rows <= LANES and heads % 4 == 0 and prop == 16
 
-    sources = (tokens, norm_gain.reshape(1, -1), w_query, w_key, w_value)
+    hbm = pl.BlockSpec(memory_space=pltpu.HBM)
+    sources = [
+        pltpu.with_memory_space_constraint(a, pltpu.HBM)
+        for a in (tokens, norm_gain.reshape(1, -1), w_query, w_key, w_value)
+    ]
     slots = pl.pallas_call(
         project_kernel,
-        out_shape=shape(heads, rows + half + 8, LANES),
-        in_specs=[pl.BlockSpec(memory_space=pltpu.HBM)] * 5,
+        out_shape=pltpu.VMEM((heads, rows + half + 8, LANES), f32),
+        in_specs=[hbm] * 5,
         out_specs=VMEM,
         scratch_shapes=[pltpu.VMEM(a.shape, a.dtype) for a in sources] + [pltpu.SemaphoreType.DMA((5,))],
         cost_estimate=pl.CostEstimate(flops=10**8, bytes_accessed=3 * MIB, transcendentals=0),
-        compiler_params=pltpu.CompilerParams(vmem_limit_bytes=67_000_000),
+        compiler_params=pltpu.CompilerParams(vmem_limit_bytes=12 * MIB),
     )(*sources)
     got = exchanged(slots, KV)
     slots, own = call(
@@ -373,25 +418,26 @@
         8,
     )(got, query_gain.reshape(1, -1), key_gain.reshape(1, -1))
     fresh = exchanged(slots, KV)
-    slots = call(
+    slots = pl.pallas_call(
         functools.partial(attend_kernel, prop),
-        shape(heads, half + prop, LANES),
-        [SMEM, SMEM, SMEM, VMEM, VMEM, VMEM],
-        4 * 10**8,
-        5 * MIB,
-        24,
+        out_shape=shape(heads, half + prop, LANES),
+        in_specs=[SMEM, SMEM, SMEM, VMEM, VMEM, VMEM],
+        out_specs=hbm,
+        scratch_shapes=[pltpu.VMEM((heads, half + prop, LANES), f32), pltpu.SemaphoreType.DMA((heads // 4,))],
+        cost_estimate=pl.CostEstimate(flops=4 * 10**8, bytes_accessed=5 * MIB, transcendentals=0),
+        compiler_params=pltpu.CompilerParams(vmem_limit_bytes=24 * MIB),
     )(base_length, accepted, head_bias, fresh, cache_keys, cache_values)
     got = exchanged(slots, KV)
-    block = pl.BlockSpec((1, span, cache_keys.shape[2]), lambda s: (s, 0, 0))
+    stored = [pltpu.with_memory_space_constraint(a, pltpu.HBM) for a in (cache_keys, cache_values)]
     tree, updated_keys, updated_values = pl.pallas_call(
         functools.partial(side_kernel, prop),
-        grid=(seqs,),
         out_shape=(shape(2, half, LANES), cache_keys, cache_values),
-        in_specs=[SMEM, SMEM, SMEM, VMEM, VMEM, VMEM, block, block],
-        out_specs=(VMEM, block, block),
+        in_specs=[SMEM, SMEM, SMEM, VMEM, VMEM, VMEM, hbm, hbm],
+        out_specs=(VMEM, hbm, hbm),
+        scratch_shapes=[pltpu.VMEM((2, *cache_keys.shape), bf16), pltpu.SemaphoreType.DMA((2, 2, seqs))],
         cost_estimate=pl.CostEstimate(flops=10**8, bytes_accessed=8 * MIB, transcendentals=0),
         compiler_params=pltpu.CompilerParams(vmem_limit_bytes=16 * MIB),
-    )(base_length, accepted, head_bias, own, parents, fresh, cache_keys, cache_values)
+    )(base_length, accepted, head_bias, own, parents, fresh, *stored)
     slots = call(combine_kernel, shape(peers, half, LANES, dtype=bf16), [VMEM] * 2, 10**7, MIB, 8)(got, tree)
     got = exchanged(slots, KV)
     part = call(output_kernel, shape(rows, columns), [VMEM] * 2, 10**8, MIB, 8)(got, w_output)

time: 81.3 us -> 78.8 us (0.969)
  local copies, waits for them, and re-layouts: 1.63 us -> 0.05 us
  Pallas kernels: 11.9 us -> 10.6 us
  waiting for transfers between devices: 4.97 us -> 6.03 us
    unnamed x20 -> x18, local copies, waits for them, and re-layouts: 1.63 us -> 0.05 us
    pallas_call x3, Pallas kernels: 10.5 us -> 9.25 us  [the longest x1 4.54 us: shards(): pl.pallas_call(functools.partial(side_kernel, prop), out_shape=(shape(2,...]
    all_to_all x1, waiting for transfers between devices: 3.73 us -> 4.79 us  [exchanged(): return lax.all_to_all(slots, axis, 0, 0, tiled=True)]
  transfers between devices with their start and end apart: 2 -> 2, of which waited for: 2 -> 2; matrix products, arithmetic and copies ran while one was open for 0% -> 0% of each run, Pallas kernels for 5% -> 6%
where the time goes in v3:
time: 78.8 us; the launch traced here: 78.4 us
  blocking collectives  57.3 us (73%)
  Pallas kernels  10.6 us (13%)
  waiting for transfers between devices  6.03 us (8%)
  starting transfers between devices  3.65 us (5%)
  between operations  0.79 us (1%)
    all_to_all x4, blocking collectives, exchanged(): return lax.all_to_all(slots, axis, 0, 0, tiled=True)  57.3 us
    all_to_all x1, waiting for transfers between devices, exchanged(): return lax.all_to_all(slots, axis, 0, 0, tiled=True)  4.79 us
    pallas_call x1, Pallas kernels, shards(): pl.pallas_call(functools.partial(side_kernel, prop), out_shape=(shape(2,...  4.54 us
    all_to_all x1, starting transfers between devices, exchanged(): return lax.all_to_all(slots, axis, 0, 0, tiled=True)  3.56 us
    pallas_call x1, Pallas kernels, shards(): pl.pallas_call(functools.partial(attend_kernel, prop), out_shape=shape(he...  2.79 us
    pallas_call x1, Pallas kernels, shards(): pl.pallas_call(project_kernel, out_shape=pltpu.VMEM((heads, rows + half +...  1.93 us
  transfers between devices with their start and end apart: 2, of which 2 were waited for; matrix products, arithmetic and copies ran while one was open for 0% of the time, Pallas kernels for 6%

profile of v3, /device:TPU:0, one launch (start us, length us, event | category | flops | bytes accessed | tf_op | source)
XLA Modules:
  0.0 78.4 jit_solution(8402293983793535711)
XLA Ops:
  0.6 0.0 copy-start.7
  0.6 0.0 copy-start.8
  0.7 1.9 %shard_map.157 = f32[16,104,128]{2,1,0:T(8,128)S(1)} custom-call(bf16[64,256]{1,0:T(8,128)(2,1)} %refs_0_.1, f32[1,256]{1,0:T(1,128)} %bitcast.5, bf16[256,1024]{1,0:T(8,128)(2,1)} %refs_2_.1, bf16[256,1024]{1,0:T(8,128)(2,1)} %refs_3_.1, bf16[256,1024]{1,0:T(8,128)(2,1)} %refs_4_.1), custom_call_target="tpu_custom_call" | custom-call | flops 100000000 | bytes 3145728 | tf_op jit(solution)/shard_map/pallas_call | solution.py:402
  2.6 23.0 %all_to_all.25.got = f32[16,104,128]{2,1,0:T(8,128)S(1)} all-to-all(f32[16,104,128]{2,1,0:T(8,128)S(1)} %shard_map.157), channel_id=1, replica_groups=mesh['dp'=4,'kv_0'=4,'kv_1'=4,'tp'=2] {'kv_0','kv_1'}, dimensions={0} | all-to-all | bytes 1703936 | tf_op jit(solution)/shard_map/all_to_all | solution.py:369
  25.6 0.0 copy-done.7
  25.6 0.0 copy-done.8
  25.6 0.0 copy-start
  25.6 0.0 copy-start.1
  25.6 0.0 copy-start.4
  25.6 0.0 copy-start.5
  25.6 0.0 copy-start.6
  25.6 0.2 shard_map.158
  25.8 12.6 %all_to_all.26.fresh = bf16[16,96,128]{2,1,0:T(8,128)(2,1)S(1)} all-to-all(bf16[16,96,128]{2,1,0:T(8,128)(2,1)S(1)} %get-tuple-element.10), channel_id=1, replica_groups=mesh['dp'=4,'kv_0'=4,'kv_1'=4,'tp'=2] {'kv_0','kv_1'}, dimensions={0} | all-to-all | bytes 786432 | tf_op jit(solution)/shard_map/all_to_all | solution.py:369
  38.4 0.0 copy-done
  38.4 0.0 copy-done.1
  38.4 0.0 copy-done.4
  38.4 0.0 copy-done.5
  38.4 0.0 copy-done.6
  38.5 0.0 copy-start.3
  38.5 2.8 %shard_map.159 = f32[16,48,128]{2,1,0:T(8,128)} custom-call(s32[4]{0:T(128)S(1)} %copy-done.4, s32[4]{0:T(128)S(1)} %copy-done.5, f32[16]{0:T(128)S(1)} %copy-done.6, bf16[16,96,128]{2,1,0:T(8,128)(2,1)S(1)} %all_to_all.26.fresh, bf16[4,256,1024]{2,1,0:T(8,128)(2,1)S(1)} %copy-done, bf16[4,256,1024]{2,1,0:T(8,128)(2,1)S(1)} %copy-done.1), custom_call_target="tpu_custom_call" | custom-call | flops 400000000 | bytes 5242880 | tf_op jit(solution)/shard_map/pallas_call | solution.py:421
  41.3 3.6 %all-to-all-start.2 = ((f32[16,48,128]{2,1,0:T(8,128)}), f32[16,48,128]{2,1,0:T(8,128)S(1)}, u32[]{:S(2)}, u32[]{:S(2)}) async-start(f32[16,48,128]{2,1,0:T(8,128)} %shard_map.159), calls=%async_computation.2 | async-start | bytes 786432 | tf_op jit(solution)/shard_map/all_to_all | solution.py:369
  44.8 0.0 copy-done.3
  44.8 0.0 copy-start.2
  44.9 4.5 %shard_map.160 = (f32[2,32,128]{2,1,0:T(8,128)S(1)}, bf16[4,256,1024]{2,1,0:T(8,128)(2,1)}, bf16[4,256,1024]{2,1,0:T(8,128)(2,1)}) custom-call(s32[4]{0:T(128)S(1)} %copy-done.4, s32[4]{0:T(128)S(1)} %copy-done.5, f32[16]{0:T(128)S(1)} %copy-done.6, bf16[96,128]{1,0:T(8,128)(2,1)S(1)} %get-tuple-element.11.own, s32[4,16]{1,0:T(4,128)S(1)} %copy-done.3, ...), custom_call_target="tpu_custom_call" | custom-call | flops 100000000 | bytes 8388608 | tf_op jit(solution)/shard_map/pallas_call | solution.py:432
  49.4 4.8 %all-to-all-done.2.got = f32[16,48,128]{2,1,0:T(8,128)S(1)} async-done(((f32[16,48,128]{2,1,0:T(8,128)}), f32[16,48,128]{2,1,0:T(8,128)S(1)}, u32[]{:S(2)}, u32[]{:S(2)}) %all-to-all-start.2) | async-done | bytes 393248 | tf_op jit(solution)/shard_map/all_to_all | solution.py:369
  54.2 0.1 shard_map.161
  54.3 10.9 %all_to_all.27.got = bf16[16,32,128]{2,1,0:T(8,128)(2,1)S(1)} all-to-all(bf16[16,32,128]{2,1,0:T(8,128)(2,1)S(1)} %shard_map.161), channel_id=1, replica_groups=mesh['dp'=4,'kv_0'=4,'kv_1'=4,'tp'=2] {'kv_0','kv_1'}, dimensions={0} | all-to-all | bytes 262144 | tf_op jit(solution)/shard_map/all_to_all | solution.py:369
  65.2 0.0 copy-done.2
  65.2 0.2 shard_map.162.one
  65.5 0.1 collective-permute-start
  65.6 1.2 %collective-permute-done.two = f32[64,256]{1,0:T(8,128)S(1)} collective-permute-done((f32[64,256]{1,0:T(8,128)S(1)}, f32[64,256]{1,0:T(8,128)S(1)}, u32[]{:S(2)}, u32[]{:S(2)}) %collective-permute-start) | collective-permute-done | bytes 65568 | tf_op jit(solution)/shard_map/ppermute | solution.py:444
  66.8 0.1 shard_map.163
  66.9 10.7 %all_to_all.28.got = f32[16,8,128]{2,1,0:T(8,128)S(1)} all-to-all(f32[16,8,128]{2,1,0:T(8,128)S(1)} %get-tuple-element.14), channel_id=1, replica_groups=mesh['dp'=4,'kv_0'=4,'kv_1'=4,'tp'=2] {'kv_0','kv_1'}, dimensions={0} | all-to-all | bytes 131072 | tf_op jit(solution)/shard_map/all_to_all | solution.py:369
  77.7 0.7 shard_map.164
Async XLA Ops:
  0.6 25.0 %copy-start.7 = (f32[64]{0:T(128)S(1)}, f32[64]{0:T(128)}, u32[]{:S(2)}) copy-start(f32[64]{0:T(128)} %param.19) | copy-start | bytes 772
  0.6 25.0 %copy-start.8 = (f32[64]{0:T(128)S(1)}, f32[64]{0:T(128)}, u32[]{:S(2)}) copy-start(f32[64]{0:T(128)} %param.20) | copy-start | bytes 772
  25.6 12.8 %copy-start = (bf16[4,256,1024]{2,1,0:T(8,128)(2,1)S(1)}, bf16[4,256,1024]{2,1,0:T(8,128)(2,1)}, u32[]{:S(2)}) copy-start(bf16[4,256,1024]{2,1,0:T(8,128)(2,1)} %keys.3) | copy-start | bytes 6291460
  25.6 12.8 %copy-start.1 = (bf16[4,256,1024]{2,1,0:T(8,128)(2,1)S(1)}, bf16[4,256,1024]{2,1,0:T(8,128)(2,1)}, u32[]{:S(2)}) copy-start(bf16[4,256,1024]{2,1,0:T(8,128)(2,1)} %values.3) | copy-start | bytes 6291460
  25.6 12.8 %copy-start.4 = (s32[4]{0:T(128)S(1)}, s32[4]{0:T(128)}, u32[]{:S(2)}) copy-start(s32[4]{0:T(128)} %base.3) | copy-start | bytes 52
  25.6 12.8 %copy-start.5 = (s32[4]{0:T(128)S(1)}, s32[4]{0:T(128)}, u32[]{:S(2)}) copy-start(s32[4]{0:T(128)} %accepted.3) | copy-start | bytes 52
  25.6 12.8 %copy-start.6 = (f32[16]{0:T(128)S(1)}, f32[16]{0:T(128)}, u32[]{:S(2)}) copy-start(f32[16]{0:T(128)} %bias.3) | copy-start | bytes 196
  38.5 6.4 %copy-start.3 = (s32[4,16]{1,0:T(4,128)S(1)}, s32[4,16]{1,0:T(4,128)}, u32[]{:S(2)}) copy-start(s32[4,16]{1,0:T(4,128)} %parents.1) | copy-start | bytes 772
  41.3 12.9 %all-to-all-start.2 = ((f32[16,48,128]{2,1,0:T(8,128)}), f32[16,48,128]{2,1,0:T(8,128)S(1)}, u32[]{:S(2)}, u32[]{:S(2)}) async-start(f32[16,48,128]{2,1,0:T(8,128)} %shard_map.159), calls=%async_computation.2 | async-start | bytes 786432 | tf_op jit(solution)/shard_map/all_to_all | solution.py:369
  44.8 20.4 %copy-start.2 = (bf16[1024,256]{1,0:T(8,128)(2,1)S(1)}, bf16[1024,256]{1,0:T(8,128)(2,1)}, u32[]{:S(2)}) copy-start(bf16[1024,256]{1,0:T(8,128)(2,1)} %w_output.1) | copy-start | bytes 1572868
  65.5 1.3 %collective-permute-start = (f32[64,256]{1,0:T(8,128)S(1)}, f32[64,256]{1,0:T(8,128)S(1)}, u32[]{:S(2)}, u32[]{:S(2)}) collective-permute-start(f32[64,256]{1,0:T(8,128)S(1)} %shard_map.162.one), channel_id=1, source_target_pairs={{0,1},{1,0},{2,3},{3,2},{4,5},{5,4},{6,7},{7,6},{8,9},{9,8},{10,11... | collective-permute-start | bytes 196616 | tf_op jit(solution)/shard_map/ppermute | solution.py:444

commit v4 on v3

--- a/solution.py
+++ b/solution.py
@@ -186,7 +186,9 @@
     order = lax.broadcasted_iota(jnp.int32, (span, span), 0)
     after = jnp.where(order > lax.broadcasted_iota(jnp.int32, (span, span), 1), 1.0, 0.0).astype(bf16)
     position = lax.axis_index(KV) * span + lax.broadcasted_iota(jnp.int32, (1, span), 1)
-    hidden = [jnp.where(position < base[seq] + accepted[seq], 0.0, HIDDEN) for seq in range(seqs)]
+    valid = base[...] + accepted[...]
+    hidden = [jnp.where(position < valid[:, seq : seq + 1], 0.0, HIDDEN) for seq in range(seqs)]
+    offset = bias[...] * LOG2_E
     quarter = lax.broadcasted_iota(jnp.int32, (prop, LANES), 1) // (LANES // seqs)
     sending = []
 
@@ -201,7 +203,7 @@
             score = dot_nt(jnp.concatenate(blocks, axis=0), stored)
             for j in range(group):
                 part = score[j * prop : (j + 1) * prop]
-                scores.append(part * (HEAD_DIM ** (-0.5) * LOG2_E) + (bias[first + j] * LOG2_E + hidden[seq]))
+                scores.append(part * (HEAD_DIM ** (-0.5) * LOG2_E) + (offset[:, first + j : first + j + 1] + hidden[seq]))
         return jnp.concatenate(scores, axis=0)
 
     def suffixes(score):
@@ -421,12 +423,12 @@
     slots = pl.pallas_call(
         functools.partial(attend_kernel, prop),
         out_shape=shape(heads, half + prop, LANES),
-        in_specs=[SMEM, SMEM, SMEM, VMEM, VMEM, VMEM],
+        in_specs=[VMEM] * 6,
         out_specs=hbm,
         scratch_shapes=[pltpu.VMEM((heads, half + prop, LANES), f32), pltpu.SemaphoreType.DMA((heads // 4,))],
         cost_estimate=pl.CostEstimate(flops=4 * 10**8, bytes_accessed=5 * MIB, transcendentals=0),
         compiler_params=pltpu.CompilerParams(vmem_limit_bytes=24 * MIB),
-    )(base_length, accepted, head_bias, fresh, cache_keys, cache_values)
+    )(*(a.reshape(1, -1) for a in (base_length, accepted, head_bias)), fresh, cache_keys, cache_values)
     got = exchanged(slots, KV)
     stored = [pltpu.with_memory_space_constraint(a, pltpu.HBM) for a in (cache_keys, cache_values)]
     tree, updated_keys, updated_values = pl.pallas_call(

time: 78.8 us -> 78.2 us (level)
  no operation moved by 1% of the time
where the time goes in v4:
time: 78.2 us; the launch traced here: 77.9 us
  blocking collectives  57.2 us (73%)
  Pallas kernels  10.1 us (13%)
  waiting for transfers between devices  6.03 us (8%)
  starting transfers between devices  3.65 us (5%)
  between operations  0.79 us (1%)
    all_to_all x4, blocking collectives, exchanged(): return lax.all_to_all(slots, axis, 0, 0, tiled=True)  57.2 us
    all_to_all x1, waiting for transfers between devices, exchanged(): return lax.all_to_all(slots, axis, 0, 0, tiled=True)  4.79 us
    pallas_call x1, Pallas kernels, shards(): pl.pallas_call(functools.partial(side_kernel, prop), out_shape=(shape(2,...  4.54 us
    all_to_all x1, starting transfers between devices, exchanged(): return lax.all_to_all(slots, axis, 0, 0, tiled=True)  3.56 us
    pallas_call x1, Pallas kernels, shards(): pl.pallas_call(functools.partial(attend_kernel, prop), out_shape=shape(he...  2.26 us
    pallas_call x1, Pallas kernels, shards(): pl.pallas_call(project_kernel, out_shape=pltpu.VMEM((heads, rows + half +...  1.93 us
  transfers between devices with their start and end apart: 2, of which 2 were waited for; matrix products, arithmetic and copies ran while one was open for 0% of the time, Pallas kernels for 6%

profile of v4, /device:TPU:0, one launch (start us, length us, event | category | flops | bytes accessed | tf_op | source)
XLA Modules:
  0.0 77.9 jit_solution(7656771878640637013)
XLA Ops:
  0.6 0.0 copy-start.7
  0.6 0.0 copy-start.8
  0.7 1.9 %shard_map.157 = f32[16,104,128]{2,1,0:T(8,128)S(1)} custom-call(bf16[64,256]{1,0:T(8,128)(2,1)} %refs_0_.1, f32[1,256]{1,0:T(1,128)} %bitcast.11, bf16[256,1024]{1,0:T(8,128)(2,1)} %refs_2_.1, bf16[256,1024]{1,0:T(8,128)(2,1)} %refs_3_.1, bf16[256,1024]{1,0:T(8,128)(2,1)} %refs_4_.1), custom_call_target="tpu_custom_call" | custom-call | flops 100000000 | bytes 3145728 | tf_op jit(solution)/shard_map/pallas_call | solution.py:404
  2.6 23.0 %all_to_all.25.got = f32[16,104,128]{2,1,0:T(8,128)S(1)} all-to-all(f32[16,104,128]{2,1,0:T(8,128)S(1)} %shard_map.157), channel_id=1, replica_groups=mesh['dp'=4,'kv_0'=4,'kv_1'=4,'tp'=2] {'kv_0','kv_1'}, dimensions={0} | all-to-all | bytes 1703936 | tf_op jit(solution)/shard_map/all_to_all | solution.py:371
  25.6 0.0 copy-done.7
  25.6 0.0 copy-done.8
  25.6 0.0 copy-start
  25.6 0.0 copy-start.1
  25.6 0.0 copy-start.4
  25.6 0.0 copy-start.5
  25.6 0.0 copy-start.6
  25.6 0.2 shard_map.158
  25.8 12.6 %all_to_all.26.fresh = bf16[16,96,128]{2,1,0:T(8,128)(2,1)S(1)} all-to-all(bf16[16,96,128]{2,1,0:T(8,128)(2,1)S(1)} %get-tuple-element.10), channel_id=1, replica_groups=mesh['dp'=4,'kv_0'=4,'kv_1'=4,'tp'=2] {'kv_0','kv_1'}, dimensions={0} | all-to-all | bytes 786432 | tf_op jit(solution)/shard_map/all_to_all | solution.py:371
  38.4 0.0 copy-done
  38.4 0.0 copy-done.1
  38.4 0.0 copy-done.4
  38.4 0.0 copy-done.5
  38.4 0.0 copy-done.6
  38.5 0.0 copy-start.3
  38.5 2.3 %shard_map.159 = f32[16,48,128]{2,1,0:T(8,128)} custom-call(s32[1,4]{1,0:T(1,128)S(1)} %bitcast.6, s32[1,4]{1,0:T(1,128)S(1)} %bitcast.7, f32[1,16]{1,0:T(1,128)S(1)} %bitcast.8, bf16[16,96,128]{2,1,0:T(8,128)(2,1)S(1)} %all_to_all.26.fresh, bf16[4,256,1024]{2,1,0:T(8,128)(2,1)S(1)} %copy-done, bf16[4,256,1024]{2,1,0:T(8,128)(2,1)S(1)} %copy-done.1), custom_call_target="tpu_custom_call" | custom-call | flops 400000000 | bytes 5242880 | tf_op jit(solution)/shard_map/pallas_call | solution.py:423
  40.7 3.6 %all-to-all-start.2 = ((f32[16,48,128]{2,1,0:T(8,128)}), f32[16,48,128]{2,1,0:T(8,128)S(1)}, u32[]{:S(2)}, u32[]{:S(2)}) async-start(f32[16,48,128]{2,1,0:T(8,128)} %shard_map.159), calls=%async_computation.2 | async-start | bytes 786432 | tf_op jit(solution)/shard_map/all_to_all | solution.py:371
  44.3 0.0 copy-done.3
  44.3 0.0 copy-start.2
  44.3 4.5 %shard_map.160 = (f32[2,32,128]{2,1,0:T(8,128)S(1)}, bf16[4,256,1024]{2,1,0:T(8,128)(2,1)}, bf16[4,256,1024]{2,1,0:T(8,128)(2,1)}) custom-call(s32[4]{0:T(128)S(1)} %copy-done.4, s32[4]{0:T(128)S(1)} %copy-done.5, f32[16]{0:T(128)S(1)} %copy-done.6, bf16[96,128]{1,0:T(8,128)(2,1)S(1)} %get-tuple-element.11.own, s32[4,16]{1,0:T(4,128)S(1)} %copy-done.3, ...), custom_call_target="tpu_custom_call" | custom-call | flops 100000000 | bytes 8388608 | tf_op jit(solution)/shard_map/pallas_call | solution.py:434
  48.9 4.8 %all-to-all-done.2.got = f32[16,48,128]{2,1,0:T(8,128)S(1)} async-done(((f32[16,48,128]{2,1,0:T(8,128)}), f32[16,48,128]{2,1,0:T(8,128)S(1)}, u32[]{:S(2)}, u32[]{:S(2)}) %all-to-all-start.2) | async-done | bytes 393248 | tf_op jit(solution)/shard_map/all_to_all | solution.py:371
  53.7 0.1 shard_map.161
  53.8 10.9 %all_to_all.27.got = bf16[16,32,128]{2,1,0:T(8,128)(2,1)S(1)} all-to-all(bf16[16,32,128]{2,1,0:T(8,128)(2,1)S(1)} %shard_map.161), channel_id=1, replica_groups=mesh['dp'=4,'kv_0'=4,'kv_1'=4,'tp'=2] {'kv_0','kv_1'}, dimensions={0} | all-to-all | bytes 262144 | tf_op jit(solution)/shard_map/all_to_all | solution.py:371
  64.7 0.0 copy-done.2
  64.7 0.2 shard_map.162.one
  65.0 0.1 collective-permute-start
  65.0 1.2 %collective-permute-done.two = f32[64,256]{1,0:T(8,128)S(1)} collective-permute-done((f32[64,256]{1,0:T(8,128)S(1)}, f32[64,256]{1,0:T(8,128)S(1)}, u32[]{:S(2)}, u32[]{:S(2)}) %collective-permute-start) | collective-permute-done | bytes 65568 | tf_op jit(solution)/shard_map/ppermute | solution.py:446
  66.3 0.1 shard_map.163
  66.4 10.7 %all_to_all.28.got = f32[16,8,128]{2,1,0:T(8,128)S(1)} all-to-all(f32[16,8,128]{2,1,0:T(8,128)S(1)} %get-tuple-element.14), channel_id=1, replica_groups=mesh['dp'=4,'kv_0'=4,'kv_1'=4,'tp'=2] {'kv_0','kv_1'}, dimensions={0} | all-to-all | bytes 131072 | tf_op jit(solution)/shard_map/all_to_all | solution.py:371
  77.1 0.7 shard_map.164
Async XLA Ops:
  0.6 25.0 %copy-start.7 = (f32[64]{0:T(128)S(1)}, f32[64]{0:T(128)}, u32[]{:S(2)}) copy-start(f32[64]{0:T(128)} %param.19) | copy-start | bytes 772
  0.6 25.0 %copy-start.8 = (f32[64]{0:T(128)S(1)}, f32[64]{0:T(128)}, u32[]{:S(2)}) copy-start(f32[64]{0:T(128)} %param.20) | copy-start | bytes 772
  25.6 12.8 %copy-start = (bf16[4,256,1024]{2,1,0:T(8,128)(2,1)S(1)}, bf16[4,256,1024]{2,1,0:T(8,128)(2,1)}, u32[]{:S(2)}) copy-start(bf16[4,256,1024]{2,1,0:T(8,128)(2,1)} %keys.3) | copy-start | bytes 6291460
  25.6 12.8 %copy-start.1 = (bf16[4,256,1024]{2,1,0:T(8,128)(2,1)S(1)}, bf16[4,256,1024]{2,1,0:T(8,128)(2,1)}, u32[]{:S(2)}) copy-start(bf16[4,256,1024]{2,1,0:T(8,128)(2,1)} %values.3) | copy-start | bytes 6291460
  25.6 12.8 %copy-start.4 = (s32[4]{0:T(128)S(1)}, s32[4]{0:T(128)}, u32[]{:S(2)}) copy-start(s32[4]{0:T(128)} %base.1) | copy-start | bytes 52
  25.6 12.8 %copy-start.5 = (s32[4]{0:T(128)S(1)}, s32[4]{0:T(128)}, u32[]{:S(2)}) copy-start(s32[4]{0:T(128)} %accepted.1) | copy-start | bytes 52
  25.6 12.8 %copy-start.6 = (f32[16]{0:T(128)S(1)}, f32[16]{0:T(128)}, u32[]{:S(2)}) copy-start(f32[16]{0:T(128)} %bias.1) | copy-start | bytes 196
  38.5 5.9 %copy-start.3 = (s32[4,16]{1,0:T(4,128)S(1)}, s32[4,16]{1,0:T(4,128)}, u32[]{:S(2)}) copy-start(s32[4,16]{1,0:T(4,128)} %parents.1) | copy-start | bytes 772
  40.7 12.9 %all-to-all-start.2 = ((f32[16,48,128]{2,1,0:T(8,128)}), f32[16,48,128]{2,1,0:T(8,128)S(1)}, u32[]{:S(2)}, u32[]{:S(2)}) async-start(f32[16,48,128]{2,1,0:T(8,128)} %shard_map.159), calls=%async_computation.2 | async-start | bytes 786432 | tf_op jit(solution)/shard_map/all_to_all | solution.py:371
  44.3 20.4 %copy-start.2 = (bf16[1024,256]{1,0:T(8,128)(2,1)S(1)}, bf16[1024,256]{1,0:T(8,128)(2,1)}, u32[]{:S(2)}) copy-start(bf16[1024,256]{1,0:T(8,128)(2,1)} %w_output.1) | copy-start | bytes 1572868
  65.0 1.3 %collective-permute-start = (f32[64,256]{1,0:T(8,128)S(1)}, f32[64,256]{1,0:T(8,128)S(1)}, u32[]{:S(2)}, u32[]{:S(2)}) collective-permute-start(f32[64,256]{1,0:T(8,128)S(1)} %shard_map.162.one), channel_id=1, source_target_pairs={{0,1},{1,0},{2,3},{3,2},{4,5},{5,4},{6,7},{7,6},{8,9},{9,8},{10,11... | collective-permute-start | bytes 196616 | tf_op jit(solution)/shard_map/ppermute | solution.py:446

commit v5 on v4

--- a/solution.py
+++ b/solution.py
@@ -14,6 +14,7 @@
 MIB = 1 << 20
 LOG2_E = 1.4426950408889634
 HIDDEN = -1e30
+CODE_BITS = 23.0
 
 epsilon = 1e-05
 f32 = jnp.float32
@@ -56,15 +57,31 @@
     return above + spill, below - spill
 
 
+def exponent(x):
+    return jnp.ceil(jnp.log2(jnp.maximum(x, 1e-30) * 1.0001))
+
+
+def coded(x, scale):
+    whole = jnp.round(x * scale).astype(jnp.int32)
+    return whole >> 8, whole & 255
+
+
 def project_kernel(*refs):
-    sources, slots, (tokens, gain, w_query, w_key, w_value), arrived = refs[:5], refs[5], refs[6:11], refs[11]
+    sources, slots, (tokens, gain, w_query, w_key, w_value), held, arrived = (
+        refs[:5],
+        refs[5],
+        refs[6:11],
+        refs[11],
+        refs[12],
+    )
     copies = [
-        pltpu.make_async_copy(source, held, arrived.at[at])
-        for at, (source, held) in enumerate(zip(sources, refs[6:11]))
+        pltpu.make_async_copy(source, target, arrived.at[at])
+        for at, (source, target) in enumerate(zip(sources, refs[6:11]))
     ]
     for copy in copies:
         copy.start()
     rows, half = tokens.shape[0], tokens.shape[0] // 2
+    tall = rows + half
     low, low_v = low_half(rows), low_half(half)
     copies[0].wait()
     wide = tokens[...].astype(f32)
@@ -72,43 +89,73 @@
     squares = jnp.concatenate((squares, jnp.zeros((LANES - rows, squares.shape[1]), f32)), axis=0)
     ones = jnp.ones((8, squares.shape[1]), bf16)
     row_squares = sum(dot_nt(ones, part) for part in split_bf16(squares, 3))
-    for head in range(slots.shape[0]):
-        slots[head, rows + half :] = row_squares
     copies[1].wait()
     scaled = (wide * gain[...]).astype(bf16)
     copies[2].wait()
     copies[3].wait()
     spans = [pl.ds(at, 2 * LANES) for at in range(0, w_query.shape[1], 2 * LANES)]
     tiles = [slice(0, LANES), slice(LANES, 2 * LANES)]
+    largest = jnp.zeros((rows, LANES), f32)
     for at, columns in enumerate(spans):
         query, key = dot(scaled, w_query[:, columns]), dot(scaled, w_key[:, columns])
         for tile, lanes in enumerate(tiles):
             head = 4 * at + 2 * tile
             q, k = query[:, lanes], turned(key[:, lanes])
-            slots[head, :rows] = jnp.where(low, q, k)
-            slots[head + 1, :rows] = jnp.where(low, k, q)
+            largest = jnp.maximum(largest, jnp.maximum(jnp.abs(q), jnp.abs(k)))
+            held[head, :rows] = jnp.where(low, q, k)
+            held[head + 1, :rows] = jnp.where(low, k, q)
     copies[4].wait()
     for at, columns in enumerate(spans):
         value = dot(scaled, w_value[:, columns])
         for tile, lanes in enumerate(tiles):
             head = 4 * at + 2 * tile
             v = value[:, lanes]
+            largest = jnp.maximum(largest, jnp.abs(v))
             v_turned = turned(v)
-            slots[head, rows : rows + half] = jnp.where(low_v, v[:half], v_turned[half:])
-            slots[head + 1, rows : rows + half] = jnp.where(low_v, v_turned[:half], v[half:])
+            held[head, rows:] = jnp.where(low_v, v[:half], v_turned[half:])
+            held[head + 1, rows:] = jnp.where(low_v, v_turned[:half], v[half:])
+    power = exponent(jnp.max(largest, axis=1, keepdims=True))
+    scale = jnp.broadcast_to(jnp.exp2(CODE_BITS - power), (rows, LANES))
+    scale = jnp.concatenate((scale, jnp.where(low_v, scale[:half], scale[half:])), axis=0)
+    lane = lax.broadcasted_iota(jnp.int32, (rows, LANES), 1)
+    row = lax.broadcasted_iota(jnp.int32, (rows, LANES), 0)
+    power = jnp.sum(jnp.where(lane == row, power, 0.0), axis=0, keepdims=True).astype(jnp.int32)
+    square_power = exponent(row_squares)
+    upper, lower = coded(row_squares, jnp.exp2(CODE_BITS - square_power))
+    line = lax.broadcasted_iota(jnp.int32, (8, LANES), 0)
+    notes = jnp.where(line == 0, power, jnp.where(line == 1, square_power.astype(jnp.int32), 0))
+    notes = jnp.where(line == 2, upper, jnp.where(line == 3, lower, notes)).astype(jnp.int16)
+    for head in range(slots.shape[0]):
+        upper, lower = coded(held[head], scale)
+        slots[head, :tall] = upper.astype(jnp.int16)
+        both = lower[: tall // 2] * 256 + lower[tall // 2 :] - 32768
+        slots[head, tall : tall + tall // 2] = both.astype(jnp.int16)
+        slots[head, tall + tall // 2 :] = notes
 
 
 def normalize_kernel(width, got, query_gain, key_gain, slots, own):
     peers = got.shape[0]
-    rows = got.shape[1] - 8
-    half = rows // 3
+    tall = (got.shape[1] - 8) // 3 * 2
+    half = tall // 3
     rows = 2 * half
     even = lax.axis_index(KV) % 2 == 0
-    total = got[0]
-    for peer in range(1, peers):
-        total = total + got[peer]
-    both, value, squares = total[:rows], total[rows : rows + half], total[rows + half : rows + half + 1]
-    low = low_half(rows)
+    low, low_v = low_half(rows), low_half(half)
+    notes = [got[peer, tall + tall // 2 :].astype(jnp.int32).astype(f32) for peer in range(peers)]
+    power, square_power, upper, lower = (
+        jnp.concatenate([note[line : line + 1] for note in notes], axis=0) for line in range(4)
+    )
+    squares = (upper * 256.0 + lower) * jnp.exp2(square_power - CODE_BITS)
+    squares = jnp.sum(squares, axis=0, keepdims=True)
+    scales = jnp.exp2(power - CODE_BITS)
+    scales = jnp.concatenate((scales, jnp.zeros((LANES - peers, LANES), f32)), axis=0).T
+    both, value = jnp.zeros((rows, LANES), f32), jnp.zeros((half, LANES), f32)
+    for peer in range(peers):
+        scale = jnp.broadcast_to(scales[:rows, peer : peer + 1], (rows, LANES))
+        pair = got[peer, tall : tall + tall // 2].astype(jnp.int32) + 32768
+        lower = jnp.concatenate((pair >> 8, pair & 255), axis=0)
+        whole = (got[peer, :tall].astype(jnp.int32) * 256 + lower).astype(f32)
+        both = both + whole[:rows] * scale
+        value = value + whole[rows:] * jnp.where(low_v, scale[:half], scale[half:])
     power = both * both
     low_sum = jnp.sum(jnp.where(low, power, 0.0), axis=1, keepdims=True)
     high_sum = jnp.sum(jnp.where(low, 0.0, power), axis=1, keepdims=True)
@@ -138,7 +185,9 @@
     other = turned(both)
     query = jnp.where(low, jnp.where(even, both, other), 0.0).astype(bf16)
     key = jnp.where(even, other, both).astype(bf16)
-    score = dot_nt(query, key) * HEAD_DIM ** (-0.5) + bias[lax.axis_index(KV)]
+    heads = lax.broadcasted_iota(jnp.int32, bias.shape, 1)
+    offset = jnp.sum(jnp.where(heads == lax.axis_index(KV), bias[...], 0.0), axis=1, keepdims=True)
+    score = dot_nt(query, key) * HEAD_DIM ** (-0.5) + offset
     row = lax.broadcasted_iota(jnp.int32, (rows, rows), 0)
     column = lax.broadcasted_iota(jnp.int32, (rows, rows), 1)
     small = [lax.broadcasted_iota(jnp.int32, (prop, prop), axis) for axis in range(2)]
@@ -189,7 +238,8 @@
     valid = base[...] + accepted[...]
     hidden = [jnp.where(position < valid[:, seq : seq + 1], 0.0, HIDDEN) for seq in range(seqs)]
     offset = bias[...] * LOG2_E
-    quarter = lax.broadcasted_iota(jnp.int32, (prop, LANES), 1) // (LANES // seqs)
+    short = prop // 2
+    eighth = lax.broadcasted_iota(jnp.int32, (short, LANES), 1) // (LANES // seqs // 2)
     sending = []
 
     def scored(at):
@@ -227,10 +277,10 @@
                 one, two = tiles[seq][rows, lanes], tiles[seq + seqs // 2][rows, lanes]
                 one, two = (one, turned(two)) if j % 2 == 0 else (turned(one), two)
                 held[head, seq * prop : (seq + 1) * prop] = jnp.where(low, one, two)
-            logs = jnp.zeros((prop, LANES), f32)
-            for seq in range(seqs):
-                start = (seq * group + j) * prop
-                logs = jnp.where(quarter == seq, log[start : start + prop], logs)
+            logs = jnp.zeros((short, LANES), f32)
+            for place in range(2 * seqs):
+                start = (place // 2 * group + j) * prop + place % 2 * short
+                logs = jnp.where(eighth == place, log[start : start + short], logs)
             held[head, half:] = logs
         chosen = pl.ds(first, group)
         copy = pltpu.make_async_copy(held.at[chosen], slots.at[chosen], sent.at[at])
@@ -250,18 +300,22 @@
 
 
 def combine_kernel(got, tree, slots):
-    blocks, tall, _ = got.shape
-    prop = tall // 3
-    half = 2 * prop
-    lane = lax.broadcasted_iota(jnp.int32, (prop, LANES), 1)
-    first = lane % HEAD_DIM < HEAD_DIM // 2
-    later = jnp.zeros((prop, LANES), f32)
+    blocks, half = got.shape[0], tree.shape[1]
+    short = half // 4
+    step = LANES // 8
+    place = lax.broadcasted_iota(jnp.int32, (short, LANES), 1) % HEAD_DIM // step
+    later = jnp.zeros((short, LANES), f32)
     part = jnp.zeros((half, LANES), f32)
     for block in range(blocks - 1, -1, -1):
         kept = jnp.exp2(-later)
-        one = jnp.where(first, kept, pltpu.roll(kept, HEAD_DIM // 2, 1))
-        two = jnp.where(first, pltpu.roll(kept, LANES - HEAD_DIM // 2, 1), kept)
-        part = part + jnp.concatenate((one, two), axis=0) * got[block, :half]
+        moved = {shift: kept if shift == 0 else pltpu.roll(kept, shift * step % LANES, 1) for shift in range(-3, 4)}
+        pieces = []
+        for wanted in range(4):
+            piece = moved[-wanted]
+            for at in range(1, 4):
+                piece = jnp.where(place == at, moved[at - wanted], piece)
+            pieces.append(piece)
+        part = part + jnp.concatenate(pieces, axis=0) * got[block, :half]
         later = later + got[block, half:]
     attended = (tree[0] + tree[1] * part).astype(bf16)
     for block in range(blocks):
@@ -319,9 +373,10 @@
     for copy in loads:
         copy.start()
     tree_part(prop, bias, own, parents, tree)
+    valid = base[...] + accepted[...]
     low = low_half(prop)
     for seq in range(seqs):
-        start = base[seq] + accepted[seq] - lax.axis_index(KV) * span
+        start = valid[0, seq] - lax.axis_index(KV) * span
         at = jnp.minimum(jnp.maximum(start, 0), span - window) // prop * prop
         lines = pl.ds(pl.multiple_of(at, prop), window)
         start = start - at
@@ -391,11 +446,13 @@
     heads = head_bias.shape[0]
     rows, span = seqs * prop, cache_keys.shape[1]
     half = rows // 2
+    tall = rows + half
     columns = w_output.shape[1]
     peers = lax.axis_size(KV)
     width = tokens.shape[1] * peers
     assert peers == heads and seqs == 4 and rows <= LANES and heads % 4 == 0 and prop == 16
 
+    lines = [a.reshape(1, -1) for a in (base_length, accepted, head_bias)]
     hbm = pl.BlockSpec(memory_space=pltpu.HBM)
     sources = [
         pltpu.with_memory_space_constraint(a, pltpu.HBM)
@@ -403,10 +460,11 @@
     ]
     slots = pl.pallas_call(
         project_kernel,
-        out_shape=pltpu.VMEM((heads, rows + half + 8, LANES), f32),
+        out_shape=pltpu.VMEM((heads, tall + tall // 2 + 8, LANES), jnp.int16),
         in_specs=[hbm] * 5,
         out_specs=VMEM,
-        scratch_shapes=[pltpu.VMEM(a.shape, a.dtype) for a in sources] + [pltpu.SemaphoreType.DMA((5,))],
+        scratch_shapes=[pltpu.VMEM(a.shape, a.dtype) for a in sources]
+        + [pltpu.VMEM((heads, tall, LANES), f32), pltpu.SemaphoreType.DMA((5,))],
         cost_estimate=pl.CostEstimate(flops=10**8, bytes_accessed=3 * MIB, transcendentals=0),
         compiler_params=pltpu.CompilerParams(vmem_limit_bytes=12 * MIB),
     )(*sources)
@@ -422,24 +480,24 @@
     fresh = exchanged(slots, KV)
     slots = pl.pallas_call(
         functools.partial(attend_kernel, prop),
-        out_shape=shape(heads, half + prop, LANES),
+        out_shape=shape(heads, half + prop // 2, LANES),
         in_specs=[VMEM] * 6,
         out_specs=hbm,
-        scratch_shapes=[pltpu.VMEM((heads, half + prop, LANES), f32), pltpu.SemaphoreType.DMA((heads // 4,))],
+        scratch_shapes=[pltpu.VMEM((heads, half + prop // 2, LANES), f32), pltpu.SemaphoreType.DMA((heads // 4,))],
         cost_estimate=pl.CostEstimate(flops=4 * 10**8, bytes_accessed=5 * MIB, transcendentals=0),
         compiler_params=pltpu.CompilerParams(vmem_limit_bytes=24 * MIB),
-    )(*(a.reshape(1, -1) for a in (base_length, accepted, head_bias)), fresh, cache_keys, cache_values)
+    )(*lines, fresh, cache_keys, cache_values)
     got = exchanged(slots, KV)
     stored = [pltpu.with_memory_space_constraint(a, pltpu.HBM) for a in (cache_keys, cache_values)]
     tree, updated_keys, updated_values = pl.pallas_call(
         functools.partial(side_kernel, prop),
         out_shape=(shape(2, half, LANES), cache_keys, cache_values),
-        in_specs=[SMEM, SMEM, SMEM, VMEM, VMEM, VMEM, hbm, hbm],
+        in_specs=[VMEM] * 6 + [hbm, hbm],
         out_specs=(VMEM, hbm, hbm),
         scratch_shapes=[pltpu.VMEM((2, *cache_keys.shape), bf16), pltpu.SemaphoreType.DMA((2, 2, seqs))],
         cost_estimate=pl.CostEstimate(flops=10**8, bytes_accessed=8 * MIB, transcendentals=0),
         compiler_params=pltpu.CompilerParams(vmem_limit_bytes=16 * MIB),
-    )(base_length, accepted, head_bias, own, parents, fresh, *stored)
+    )(*lines, own, parents, fresh, *stored)
     slots = call(combine_kernel, shape(peers, half, LANES, dtype=bf16), [VMEM] * 2, 10**7, MIB, 8)(got, tree)
     got = exchanged(slots, KV)
     part = call(output_kernel, shape(rows, columns), [VMEM] * 2, 10**8, MIB, 8)(got, w_output)

time: 78.2 us -> 76 us (0.972)
  blocking collectives: 57.2 us -> 54.8 us
    all_to_all x4, blocking collectives: 57.2 us -> 54.8 us  [exchanged(): return lax.all_to_all(slots, axis, 0, 0, tiled=True)]
where the time goes in v5:
time: 76 us; the launch traced here: 75.6 us
  blocking collectives  54.8 us (72%)
  Pallas kernels  10.4 us (14%)
  waiting for transfers between devices  6 us (8%)
  starting transfers between devices  3.64 us (5%)
  between operations  0.79 us (1%)
    all_to_all x4, blocking collectives, exchanged(): return lax.all_to_all(slots, axis, 0, 0, tiled=True)  54.8 us
    all_to_all x1, waiting for transfers between devices, exchanged(): return lax.all_to_all(slots, axis, 0, 0, tiled=True)  4.76 us
    pallas_call x1, Pallas kernels, shards(): pl.pallas_call(functools.partial(side_kernel, prop), out_shape=(shape(2,...  4.21 us
    all_to_all x1, starting transfers between devices, exchanged(): return lax.all_to_all(slots, axis, 0, 0, tiled=True)  3.55 us
    pallas_call x1, Pallas kernels, shards(): pl.pallas_call(functools.partial(attend_kernel, prop), out_shape=shape(he...  2.25 us
    pallas_call x1, Pallas kernels, shards(): pl.pallas_call(project_kernel, out_shape=pltpu.VMEM((heads, tall + tall /...  2.17 us
  transfers between devices with their start and end apart: 2, of which 2 were waited for; matrix products, arithmetic and copies ran while one was open for 0% of the time, Pallas kernels for 6%

profile of v5, /device:TPU:0, one launch (start us, length us, event | category | flops | bytes accessed | tf_op | source)
XLA Modules:
  0.0 75.6 jit_solution(14009158162979579993)
XLA Ops:
  0.6 0.0 copy-start.7
  0.6 0.0 copy-start.8
  0.7 2.2 %shard_map.157 = s16[16,152,128]{2,1,0:T(8,128)(2,1)S(1)} custom-call(bf16[64,256]{1,0:T(8,128)(2,1)} %refs_0_.1, f32[1,256]{1,0:T(1,128)} %bitcast.14, bf16[256,1024]{1,0:T(8,128)(2,1)} %refs_2_.1, bf16[256,1024]{1,0:T(8,128)(2,1)} %refs_3_.1, bf16[256,1024]{1,0:T(8,128)(2,1)} %refs_4_.1), custom_call_target="tpu_custom_call" | custom-call | flops 100000000 | bytes 3145728 | tf_op jit(solution)/shard_map/pallas_call | solution.py:461
  2.8 20.5 %all_to_all.25.got = s16[16,152,128]{2,1,0:T(8,128)(2,1)S(1)} all-to-all(s16[16,152,128]{2,1,0:T(8,128)(2,1)S(1)} %shard_map.157), channel_id=1, replica_groups=mesh['dp'=4,'kv_0'=4,'kv_1'=4,'tp'=2] {'kv_0','kv_1'}, dimensions={0} | all-to-all | bytes 1245184 | tf_op jit(solution)/shard_map/all_to_all | solution.py:426
  23.4 0.0 copy-done.7
  23.4 0.0 copy-done.8
  23.4 0.0 copy-start
  23.4 0.0 copy-start.1
  23.4 0.0 copy-start.4
  23.4 0.0 copy-start.5
  23.4 0.0 copy-start.6
  23.4 0.5 shard_map.158
  23.9 12.6 %all_to_all.26.fresh = bf16[16,96,128]{2,1,0:T(8,128)(2,1)S(1)} all-to-all(bf16[16,96,128]{2,1,0:T(8,128)(2,1)S(1)} %get-tuple-element.10), channel_id=1, replica_groups=mesh['dp'=4,'kv_0'=4,'kv_1'=4,'tp'=2] {'kv_0','kv_1'}, dimensions={0} | all-to-all | bytes 786432 | tf_op jit(solution)/shard_map/all_to_all | solution.py:426
  36.6 0.0 copy-done
  36.6 0.0 copy-done.1
  36.6 0.0 copy-done.4
  36.6 0.0 copy-done.5
  36.6 0.0 copy-done.6
  36.6 0.0 copy-start.3
  36.6 2.2 %shard_map.159 = f32[16,40,128]{2,1,0:T(8,128)} custom-call(s32[1,4]{1,0:T(1,128)S(1)} %bitcast.6, s32[1,4]{1,0:T(1,128)S(1)} %bitcast.8, f32[1,16]{1,0:T(1,128)S(1)} %bitcast.10, bf16[16,96,128]{2,1,0:T(8,128)(2,1)S(1)} %all_to_all.26.fresh, bf16[4,256,1024]{2,1,0:T(8,128)(2,1)S(1)} %copy-done, bf16[4,256,1024]{2,1,0:T(8,128)(2,1)S(1)} %copy-done.1), custom_call_target="tpu_custom_call" | custom-call | flops 400000000 | bytes 5242880 | tf_op jit(solution)/shard_map/pallas_call | solution.py:481
  38.9 3.6 %all-to-all-start.2 = ((f32[16,40,128]{2,1,0:T(8,128)}), f32[16,40,128]{2,1,0:T(8,128)S(1)}, u32[]{:S(2)}, u32[]{:S(2)}) async-start(f32[16,40,128]{2,1,0:T(8,128)} %shard_map.159), calls=%async_computation.2 | async-start | bytes 655360 | tf_op jit(solution)/shard_map/all_to_all | solution.py:426
  42.4 0.0 copy-done.3
  42.4 0.0 copy-start.2
  42.4 4.2 %shard_map.160 = (f32[2,32,128]{2,1,0:T(8,128)S(1)}, bf16[4,256,1024]{2,1,0:T(8,128)(2,1)}, bf16[4,256,1024]{2,1,0:T(8,128)(2,1)}) custom-call(s32[1,4]{1,0:T(1,128)S(1)} %bitcast.7, s32[1,4]{1,0:T(1,128)S(1)} %bitcast.9, f32[1,16]{1,0:T(1,128)S(1)} %bitcast.11, bf16[96,128]{1,0:T(8,128)(2,1)S(1)} %get-tuple-element.11.own, s32[4,16]{1,0:T(4,128)S(1)} %copy-done.3, ...), custom_call_target="tpu_custom_call" | custom-call | flops 100000000 | bytes 8388608 | tf_op jit(solution)/shard_map/pallas_call | solution.py:492
  46.7 4.8 %all-to-all-done.2.got = f32[16,40,128]{2,1,0:T(8,128)S(1)} async-done(((f32[16,40,128]{2,1,0:T(8,128)}), f32[16,40,128]{2,1,0:T(8,128)S(1)}, u32[]{:S(2)}, u32[]{:S(2)}) %all-to-all-start.2) | async-done | bytes 327712 | tf_op jit(solution)/shard_map/all_to_all | solution.py:426
  51.4 0.2 shard_map.161
  51.6 10.8 %all_to_all.27.got = bf16[16,32,128]{2,1,0:T(8,128)(2,1)S(1)} all-to-all(bf16[16,32,128]{2,1,0:T(8,128)(2,1)S(1)} %shard_map.161), channel_id=1, replica_groups=mesh['dp'=4,'kv_0'=4,'kv_1'=4,'tp'=2] {'kv_0','kv_1'}, dimensions={0} | all-to-all | bytes 262144 | tf_op jit(solution)/shard_map/all_to_all | solution.py:426
  62.4 0.0 copy-done.2
  62.4 0.2 shard_map.162.one
  62.7 0.1 collective-permute-start
  62.8 1.2 %collective-permute-done.two = f32[64,256]{1,0:T(8,128)S(1)} collective-permute-done((f32[64,256]{1,0:T(8,128)S(1)}, f32[64,256]{1,0:T(8,128)S(1)}, u32[]{:S(2)}, u32[]{:S(2)}) %collective-permute-start) | collective-permute-done | bytes 65568 | tf_op jit(solution)/shard_map/ppermute | solution.py:504
  64.0 0.1 shard_map.163
  64.1 10.7 %all_to_all.28.got = f32[16,8,128]{2,1,0:T(8,128)S(1)} all-to-all(f32[16,8,128]{2,1,0:T(8,128)S(1)} %get-tuple-element.14), channel_id=1, replica_groups=mesh['dp'=4,'kv_0'=4,'kv_1'=4,'tp'=2] {'kv_0','kv_1'}, dimensions={0} | all-to-all | bytes 131072 | tf_op jit(solution)/shard_map/all_to_all | solution.py:426
  74.9 0.7 shard_map.164
Async XLA Ops:
  0.6 22.7 %copy-start.7 = (f32[64]{0:T(128)S(1)}, f32[64]{0:T(128)}, u32[]{:S(2)}) copy-start(f32[64]{0:T(128)} %param.19) | copy-start | bytes 772
  0.6 22.7 %copy-start.8 = (f32[64]{0:T(128)S(1)}, f32[64]{0:T(128)}, u32[]{:S(2)}) copy-start(f32[64]{0:T(128)} %param.20) | copy-start | bytes 772
  23.4 13.2 %copy-start = (bf16[4,256,1024]{2,1,0:T(8,128)(2,1)S(1)}, bf16[4,256,1024]{2,1,0:T(8,128)(2,1)}, u32[]{:S(2)}) copy-start(bf16[4,256,1024]{2,1,0:T(8,128)(2,1)} %keys.3) | copy-start | bytes 6291460
  23.4 13.2 %copy-start.1 = (bf16[4,256,1024]{2,1,0:T(8,128)(2,1)S(1)}, bf16[4,256,1024]{2,1,0:T(8,128)(2,1)}, u32[]{:S(2)}) copy-start(bf16[4,256,1024]{2,1,0:T(8,128)(2,1)} %values.3) | copy-start | bytes 6291460
  23.4 13.2 %copy-start.4 = (s32[4]{0:T(128)S(1)}, s32[4]{0:T(128)}, u32[]{:S(2)}) copy-start(s32[4]{0:T(128)} %param.25) | copy-start | bytes 52
  23.4 13.2 %copy-start.5 = (s32[4]{0:T(128)S(1)}, s32[4]{0:T(128)}, u32[]{:S(2)}) copy-start(s32[4]{0:T(128)} %param.26) | copy-start | bytes 52
  23.4 13.2 %copy-start.6 = (f32[16]{0:T(128)S(1)}, f32[16]{0:T(128)}, u32[]{:S(2)}) copy-start(f32[16]{0:T(128)} %param.21) | copy-start | bytes 196
  36.6 5.8 %copy-start.3 = (s32[4,16]{1,0:T(4,128)S(1)}, s32[4,16]{1,0:T(4,128)}, u32[]{:S(2)}) copy-start(s32[4,16]{1,0:T(4,128)} %parents.1) | copy-start | bytes 772
  38.9 12.6 %all-to-all-start.2 = ((f32[16,40,128]{2,1,0:T(8,128)}), f32[16,40,128]{2,1,0:T(8,128)S(1)}, u32[]{:S(2)}, u32[]{:S(2)}) async-start(f32[16,40,128]{2,1,0:T(8,128)} %shard_map.159), calls=%async_computation.2 | async-start | bytes 655360 | tf_op jit(solution)/shard_map/all_to_all | solution.py:426
  42.4 20.0 %copy-start.2 = (bf16[1024,256]{1,0:T(8,128)(2,1)S(1)}, bf16[1024,256]{1,0:T(8,128)(2,1)}, u32[]{:S(2)}) copy-start(bf16[1024,256]{1,0:T(8,128)(2,1)} %w_output.1) | copy-start | bytes 1572868
  62.7 1.3 %collective-permute-start = (f32[64,256]{1,0:T(8,128)S(1)}, f32[64,256]{1,0:T(8,128)S(1)}, u32[]{:S(2)}, u32[]{:S(2)}) collective-permute-start(f32[64,256]{1,0:T(8,128)S(1)} %shard_map.162.one), channel_id=1, source_target_pairs={{0,1},{1,0},{2,3},{3,2},{4,5},{5,4},{6,7},{7,6},{8,9},{9,8},{10,11... | collective-permute-start | bytes 196616 | tf_op jit(solution)/shard_map/ppermute | solution.py:504

commit v6 on v5

--- a/solution.py
+++ b/solution.py
@@ -503,7 +503,7 @@
     part = call(output_kernel, shape(rows, columns), [VMEM] * 2, 10**8, MIB, 8)(got, w_output)
     other = lax.ppermute(part, "tp", [(0, 1), (1, 0)])
     mix, slots = call(
-        squares_kernel, (shape(rows, columns), shape(peers, 8, LANES)), [VMEM] * 2, 10**6, MIB // 4, 4
+        squares_kernel, (shape(rows, columns), shape(peers, 1, LANES)), [VMEM] * 2, 10**6, MIB // 4, 4
     )(part, other)
     got = exchanged(slots, KV)
     layer_out = call(

time: 76 us -> 75.9 us (level)
  no operation moved by 1% of the time
where the time goes in v6:
time: 75.9 us; the launch traced here: 75.5 us
  blocking collectives  54.7 us (72%)
  Pallas kernels  10.4 us (14%)
  waiting for transfers between devices  6 us (8%)
  starting transfers between devices  3.64 us (5%)
  between operations  0.79 us (1%)
    all_to_all x4, blocking collectives, exchanged(): return lax.all_to_all(slots, axis, 0, 0, tiled=True)  54.7 us
    all_to_all x1, waiting for transfers between devices, exchanged(): return lax.all_to_all(slots, axis, 0, 0, tiled=True)  4.76 us
    pallas_call x1, Pallas kernels, shards(): pl.pallas_call(functools.partial(side_kernel, prop), out_shape=(shape(2,...  4.21 us
    all_to_all x1, starting transfers between devices, exchanged(): return lax.all_to_all(slots, axis, 0, 0, tiled=True)  3.55 us
    pallas_call x1, Pallas kernels, shards(): pl.pallas_call(functools.partial(attend_kernel, prop), out_shape=shape(he...  2.25 us
    pallas_call x1, Pallas kernels, shards(): pl.pallas_call(project_kernel, out_shape=pltpu.VMEM((heads, tall + tall /...  2.17 us
  transfers between devices with their start and end apart: 2, of which 2 were waited for; matrix products, arithmetic and copies ran while one was open for 0% of the time, Pallas kernels for 6%

profile of v6, /device:TPU:0, one launch (start us, length us, event | category | flops | bytes accessed | tf_op | source)
XLA Modules:
  0.0 75.5 jit_solution(13494981830817610482)
XLA Ops:
  0.6 0.0 copy-start.7
  0.6 0.0 copy-start.8
  0.7 2.2 %shard_map.157 = s16[16,152,128]{2,1,0:T(8,128)(2,1)S(1)} custom-call(bf16[64,256]{1,0:T(8,128)(2,1)} %refs_0_.1, f32[1,256]{1,0:T(1,128)} %bitcast.14, bf16[256,1024]{1,0:T(8,128)(2,1)} %refs_2_.1, bf16[256,1024]{1,0:T(8,128)(2,1)} %refs_3_.1, bf16[256,1024]{1,0:T(8,128)(2,1)} %refs_4_.1), custom_call_target="tpu_custom_call" | custom-call | flops 100000000 | bytes 3145728 | tf_op jit(solution)/shard_map/pallas_call | solution.py:461
  2.8 20.5 %all_to_all.25.got = s16[16,152,128]{2,1,0:T(8,128)(2,1)S(1)} all-to-all(s16[16,152,128]{2,1,0:T(8,128)(2,1)S(1)} %shard_map.157), channel_id=1, replica_groups=mesh['dp'=4,'kv_0'=4,'kv_1'=4,'tp'=2] {'kv_0','kv_1'}, dimensions={0} | all-to-all | bytes 1245184 | tf_op jit(solution)/shard_map/all_to_all | solution.py:426
  23.4 0.0 copy-done.7
  23.4 0.0 copy-done.8
  23.4 0.0 copy-start
  23.4 0.0 copy-start.1
  23.4 0.0 copy-start.4
  23.4 0.0 copy-start.5
  23.4 0.0 copy-start.6
  23.4 0.5 shard_map.158
  23.9 12.6 %all_to_all.26.fresh = bf16[16,96,128]{2,1,0:T(8,128)(2,1)S(1)} all-to-all(bf16[16,96,128]{2,1,0:T(8,128)(2,1)S(1)} %get-tuple-element.10), channel_id=1, replica_groups=mesh['dp'=4,'kv_0'=4,'kv_1'=4,'tp'=2] {'kv_0','kv_1'}, dimensions={0} | all-to-all | bytes 786432 | tf_op jit(solution)/shard_map/all_to_all | solution.py:426
  36.6 0.0 copy-done
  36.6 0.0 copy-done.1
  36.6 0.0 copy-done.4
  36.6 0.0 copy-done.5
  36.6 0.0 copy-done.6
  36.6 0.0 copy-start.3
  36.6 2.2 %shard_map.159 = f32[16,40,128]{2,1,0:T(8,128)} custom-call(s32[1,4]{1,0:T(1,128)S(1)} %bitcast.6, s32[1,4]{1,0:T(1,128)S(1)} %bitcast.8, f32[1,16]{1,0:T(1,128)S(1)} %bitcast.10, bf16[16,96,128]{2,1,0:T(8,128)(2,1)S(1)} %all_to_all.26.fresh, bf16[4,256,1024]{2,1,0:T(8,128)(2,1)S(1)} %copy-done, bf16[4,256,1024]{2,1,0:T(8,128)(2,1)S(1)} %copy-done.1), custom_call_target="tpu_custom_call" | custom-call | flops 400000000 | bytes 5242880 | tf_op jit(solution)/shard_map/pallas_call | solution.py:481
  38.9 3.6 %all-to-all-start.2 = ((f32[16,40,128]{2,1,0:T(8,128)}), f32[16,40,128]{2,1,0:T(8,128)S(1)}, u32[]{:S(2)}, u32[]{:S(2)}) async-start(f32[16,40,128]{2,1,0:T(8,128)} %shard_map.159), calls=%async_computation.2 | async-start | bytes 655360 | tf_op jit(solution)/shard_map/all_to_all | solution.py:426
  42.4 0.0 copy-done.3
  42.4 0.0 copy-start.2
  42.4 4.2 %shard_map.160 = (f32[2,32,128]{2,1,0:T(8,128)S(1)}, bf16[4,256,1024]{2,1,0:T(8,128)(2,1)}, bf16[4,256,1024]{2,1,0:T(8,128)(2,1)}) custom-call(s32[1,4]{1,0:T(1,128)S(1)} %bitcast.7, s32[1,4]{1,0:T(1,128)S(1)} %bitcast.9, f32[1,16]{1,0:T(1,128)S(1)} %bitcast.11, bf16[96,128]{1,0:T(8,128)(2,1)S(1)} %get-tuple-element.11.own, s32[4,16]{1,0:T(4,128)S(1)} %copy-done.3, ...), custom_call_target="tpu_custom_call" | custom-call | flops 100000000 | bytes 8388608 | tf_op jit(solution)/shard_map/pallas_call | solution.py:492
  46.7 4.8 %all-to-all-done.2.got = f32[16,40,128]{2,1,0:T(8,128)S(1)} async-done(((f32[16,40,128]{2,1,0:T(8,128)}), f32[16,40,128]{2,1,0:T(8,128)S(1)}, u32[]{:S(2)}, u32[]{:S(2)}) %all-to-all-start.2) | async-done | bytes 327712 | tf_op jit(solution)/shard_map/all_to_all | solution.py:426
  51.4 0.2 shard_map.161
  51.6 10.8 %all_to_all.27.got = bf16[16,32,128]{2,1,0:T(8,128)(2,1)S(1)} all-to-all(bf16[16,32,128]{2,1,0:T(8,128)(2,1)S(1)} %shard_map.161), channel_id=1, replica_groups=mesh['dp'=4,'kv_0'=4,'kv_1'=4,'tp'=2] {'kv_0','kv_1'}, dimensions={0} | all-to-all | bytes 262144 | tf_op jit(solution)/shard_map/all_to_all | solution.py:426
  62.4 0.0 copy-done.2
  62.4 0.2 shard_map.162.one
  62.7 0.1 collective-permute-start
  62.8 1.2 %collective-permute-done.two = f32[64,256]{1,0:T(8,128)S(1)} collective-permute-done((f32[64,256]{1,0:T(8,128)S(1)}, f32[64,256]{1,0:T(8,128)S(1)}, u32[]{:S(2)}, u32[]{:S(2)}) %collective-permute-start) | collective-permute-done | bytes 65568 | tf_op jit(solution)/shard_map/ppermute | solution.py:504
  64.0 0.1 shard_map.163
  64.1 10.7 %all_to_all.28.got = f32[16,1,128]{2,1,0:T(1,128)S(1)} all-to-all(f32[16,1,128]{2,1,0:T(1,128)S(1)} %get-tuple-element.14), channel_id=1, replica_groups=mesh['dp'=4,'kv_0'=4,'kv_1'=4,'tp'=2] {'kv_0','kv_1'}, dimensions={0} | all-to-all | bytes 16384 | tf_op jit(solution)/shard_map/all_to_all | solution.py:426
  74.8 0.7 shard_map.164
Async XLA Ops:
  0.6 22.7 %copy-start.7 = (f32[64]{0:T(128)S(1)}, f32[64]{0:T(128)}, u32[]{:S(2)}) copy-start(f32[64]{0:T(128)} %param.19) | copy-start | bytes 772
  0.6 22.7 %copy-start.8 = (f32[64]{0:T(128)S(1)}, f32[64]{0:T(128)}, u32[]{:S(2)}) copy-start(f32[64]{0:T(128)} %param.20) | copy-start | bytes 772
  23.4 13.2 %copy-start = (bf16[4,256,1024]{2,1,0:T(8,128)(2,1)S(1)}, bf16[4,256,1024]{2,1,0:T(8,128)(2,1)}, u32[]{:S(2)}) copy-start(bf16[4,256,1024]{2,1,0:T(8,128)(2,1)} %keys.3) | copy-start | bytes 6291460
  23.4 13.2 %copy-start.1 = (bf16[4,256,1024]{2,1,0:T(8,128)(2,1)S(1)}, bf16[4,256,1024]{2,1,0:T(8,128)(2,1)}, u32[]{:S(2)}) copy-start(bf16[4,256,1024]{2,1,0:T(8,128)(2,1)} %values.3) | copy-start | bytes 6291460
  23.4 13.2 %copy-start.4 = (s32[4]{0:T(128)S(1)}, s32[4]{0:T(128)}, u32[]{:S(2)}) copy-start(s32[4]{0:T(128)} %param.25) | copy-start | bytes 52
  23.4 13.2 %copy-start.5 = (s32[4]{0:T(128)S(1)}, s32[4]{0:T(128)}, u32[]{:S(2)}) copy-start(s32[4]{0:T(128)} %param.26) | copy-start | bytes 52
  23.4 13.2 %copy-start.6 = (f32[16]{0:T(128)S(1)}, f32[16]{0:T(128)}, u32[]{:S(2)}) copy-start(f32[16]{0:T(128)} %param.21) | copy-start | bytes 196
  36.6 5.8 %copy-start.3 = (s32[4,16]{1,0:T(4,128)S(1)}, s32[4,16]{1,0:T(4,128)}, u32[]{:S(2)}) copy-start(s32[4,16]{1,0:T(4,128)} %parents.1) | copy-start | bytes 772
  38.9 12.6 %all-to-all-start.2 = ((f32[16,40,128]{2,1,0:T(8,128)}), f32[16,40,128]{2,1,0:T(8,128)S(1)}, u32[]{:S(2)}, u32[]{:S(2)}) async-start(f32[16,40,128]{2,1,0:T(8,128)} %shard_map.159), calls=%async_computation.2 | async-start | bytes 655360 | tf_op jit(solution)/shard_map/all_to_all | solution.py:426
  42.4 20.0 %copy-start.2 = (bf16[1024,256]{1,0:T(8,128)(2,1)S(1)}, bf16[1024,256]{1,0:T(8,128)(2,1)}, u32[]{:S(2)}) copy-start(bf16[1024,256]{1,0:T(8,128)(2,1)} %w_output.1) | copy-start | bytes 1572868
  62.7 1.3 %collective-permute-start = (f32[64,256]{1,0:T(8,128)S(1)}, f32[64,256]{1,0:T(8,128)S(1)}, u32[]{:S(2)}, u32[]{:S(2)}) collective-permute-start(f32[64,256]{1,0:T(8,128)S(1)} %shard_map.162.one), channel_id=1, source_target_pairs={{0,1},{1,0},{2,3},{3,2},{4,5},{5,4},{6,7},{7,6},{8,9},{9,8},{10,11... | collective-permute-start | bytes 196616 | tf_op jit(solution)/shard_map/ppermute | solution.py:504
